TPU v7x, 32 devices: a whole 2x2x4 slice. The times are simulated.
32 devices in a mesh: ep: 8 (over z, y), tp: 4 (over x, core).
Axes of the slice: x: 2, y: 2, z: 4, core: 2. Of those that a mesh axis runs over, the one named last changes fastest.
Arguments:
- tokens: bfloat16 [128, 4096], P(None, 'ep'), may hold values from -80 to 80
- mix_gain: bfloat16 [4096], P('ep'), may hold values from 0.099609375 to 1.8984375
- w_query: bfloat16 [4096, 1024], P('ep', 'tp'), may hold values from -0.09375 to 0.09375
- w_key: bfloat16 [4096, 1024], P('ep', 'tp'), may hold values from -0.09375 to 0.09375
- w_value: bfloat16 [4096, 2048], P('ep', 'tp'), may hold values from -0.09375 to 0.09375
- w_outgate: bfloat16 [4096, 2048], P('ep', 'tp'), may hold values from -0.09375 to 0.09375
- w_igate: bfloat16 [4096, 16], P('ep', 'tp'), may hold values from -0.09375 to 0.09375
- w_fgate: bfloat16 [4096, 16], P('ep', 'tp'), may hold values from -0.09375 to 0.09375
- igate_bias: float32 [16], P('tp'), may hold values from -3 to 3
- fgate_bias: float32 [16], P('tp'), may hold values from -1 to 3
- head_gain: bfloat16 [2048], P('tp'), may hold values from 0.099609375 to 1.8984375
- w_mixout: bfloat16 [2048, 4096], P('tp', 'ep'), may hold values from -0.125 to 0.125
- state_matrix: float32 [128, 16, 64, 128], P('ep', 'tp'), may hold values from -3 to 3
- state_norm: float32 [128, 16, 64], P('ep', 'tp'), may hold values from -3 to 3
- state_max: float32 [128, 16], P('ep', 'tp'), may hold values from -3 to 3
- ffn_gain: bfloat16 [4096], P('ep'), may hold values from 0.099609375 to 1.8984375
- dense_mix: bfloat16 [4096], P('ep'), may hold values from -0.09375 to 0.09375
- w_dense_gate: bfloat16 [4096, 1024], P('ep', 'tp'), may hold values from -0.09375 to 0.09375
- w_dense_up: bfloat16 [4096, 1024], P('ep', 'tp'), may hold values from -0.09375 to 0.09375
- w_dense_down: bfloat16 [1024, 4096], P('tp', 'ep'), may hold values from -0.1875 to 0.1875
- routes: int32 [128, 4], replicated, may hold values from 0 to 7, all different within a row; in each aligned block of 16 rows (0 to 15, 16 to 31, ...) at most 16 rows name the same one
- route_weights: float32 [128, 4], replicated, may hold values from 0.2 to 1.5
- w_exp_gate: bfloat16 [8, 4096, 1024], P('ep', None, 'tp'), may hold values from -0.09375 to 0.09375
- w_exp_up: bfloat16 [8, 4096, 1024], P('ep', None, 'tp'), may hold values from -0.09375 to 0.09375
- w_exp_down: bfloat16 [8, 1024, 4096], P('ep', 'tp'), may hold values from -0.1875 to 0.1875
Outputs:
- layer_out: bfloat16 [128, 4096], P(None, 'ep')
- new_matrix: float32 [128, 16, 64, 128], P('ep', 'tp')
- new_norm: float32 [128, 16, 64], P('ep', 'tp')
- new_max: float32 [128, 16], P('ep', 'tp')
Inputs may be any that keep to these rules, and one draw needn't show every extreme that they name: `routes`: each row names 4 different experts. In the rows of one device (aligned blocks of 16 rows) no expert is named by more than 16 rows, a bound that some block reaches.
All inputs are finite; a program needn't handle non-finite values.
Results may differ from a plain program's by a relative error of at most 0.012.
Values may be sent and summed in bfloat16 or wider, within the bound.
A program may use at most 128 MiB of HBM per device.

v0:
```python
import functools

import jax
import jax.numpy as jnp
from jax import lax
from jax.experimental import pallas as pl
from jax.experimental.pallas import tpu as pltpu
from jax.sharding import PartitionSpec as P

EPSILON = 1e-06
SOFT_CAP = 15.0
MESH = pl.DeviceIdType.MESH
F32 = jnp.float32
BF16 = jnp.bfloat16


def each(count, body):
    if count <= 8:
        for i in range(count):
            body(i)
    else:

        @pl.loop(0, count)
        def _(i):
            body(i)


def dot(a, b):
    return jnp.dot(a, b, preferred_element_type=F32)


def pick_lane(x, lane):
    lanes = lax.broadcasted_iota(jnp.int32, x.shape, 1)
    return jnp.sum(jnp.where(lanes == lane, x, 0.0), axis=1, keepdims=True)


def layer_kernel(
    n,
    tn,
    d_model,
    tokens,
    small,
    w_gates,
    state_norm,
    state_max,
    routes,
    route_weights,
    w_query,
    w_key,
    w_value,
    w_outgate,
    w_mixout,
    state_matrix,
    w_dense_gate,
    w_dense_up,
    w_dense_down,
    w_exp_gate,
    w_exp_up,
    w_exp_down,
    layer_out,
    new_matrix,
    new_norm,
    new_max,
    wq,
    wk,
    wv,
    wo,
    wm,
    sm,
    wdg,
    wdu,
    wdd,
    weg,
    weu,
    wed,
    proj_send,
    proj_recv,
    gate_send,
    gate_recv,
    num,
    heads_all,
    mix_send,
    mix_recv,
    hid_own,
    y_all,
    stat_send,
    stat_recv,
    stat_all,
    inv_two,
    dense_send,
    dense_recv,
    unit_all,
    exp_acc,
    near_recv,
    far_recv,
    res_recv,
    out_acc,
    fin_send,
    fin_recv,
    fin_all,
    norm_wide,
    square,
    local_sem,
    down_sem,
    ep_send,
    ep_recv,
    tp_send,
    tp_recv,
    pair_send,
    pair_recv,
):
    me = lax.axis_index("ep")
    mt = lax.axis_index("tp")
    rows, feats = tokens.shape
    chunk = min(rows, 128)
    chunks = rows // chunk
    seqs = state_norm.shape[0]
    heads, dk, dv = sm.shape[1], sm.shape[2], sm.shape[3]
    hk, hv = heads * dk, heads * dv
    units = wdg.shape[1]
    quarter = rows // tn
    per_chunk = chunk // seqs

    def fetch(i, src, dst):
        copy = pltpu.make_async_copy(src, dst, local_sem.at[i])
        copy.start()
        return copy

    in_q = fetch(0, w_query, wq)
    in_k = fetch(1, w_key, wk)
    in_v = fetch(2, w_value, wv)
    in_o = fetch(3, w_outgate, wo)
    in_s = fetch(4, state_matrix, sm)
    in_m = fetch(5, w_mixout, wm)
    in_dg = fetch(6, w_dense_gate, wdg)
    in_du = fetch(7, w_dense_up, wdu)
    in_dd = fetch(8, w_dense_down, wdd)
    in_eg = fetch(9, w_exp_gate.at[0], weg)
    in_eu = fetch(10, w_exp_up.at[0], weu)

    def down_copy(t):
        if w_exp_down.shape[2] == n * feats:
            src = w_exp_down.at[0, :, pl.ds(pl.multiple_of(t * feats, 128), feats)]
        else:
            src = w_exp_down.at[t]
        return pltpu.make_async_copy(src, wed.at[t], down_sem.at[t])

    each(n, lambda t: down_copy(t).start())

    def ep_copy(phase, k, src, dst):
        return pltpu.make_async_remote_copy(
            src_ref=src,
            dst_ref=dst,
            send_sem=ep_send.at[phase, k - 1],
            recv_sem=ep_recv.at[phase, k - 1],
            device_id={"ep": lax.rem(me + k, n)},
            device_id_type=MESH,
        )

    def tp_copy(phase, k, src, dst):
        return pltpu.make_async_remote_copy(
            src_ref=src,
            dst_ref=dst,
            send_sem=tp_send.at[phase, k - 1],
            recv_sem=tp_recv.at[phase, k - 1],
            device_id={"tp": lax.rem(mt + k, tn)},
            device_id_type=MESH,
        )

    def peers(body):
        each(n - 1, lambda i: body(i + 1))

    def tp_peers(body):
        each(tn - 1, lambda i: body(i + 1))

    barrier = pltpu.get_barrier_semaphore()
    peers(
        lambda k: pl.semaphore_signal(
            barrier, inc=1, device_id={"ep": lax.rem(me + k, n)}, device_id_type=MESH
        )
    )
    tp_peers(
        lambda k: pl.semaphore_signal(
            barrier, inc=1, device_id={"tp": lax.rem(mt + k, tn)}, device_id_type=MESH
        )
    )

    def row_slice(c):
        return pl.ds(pl.multiple_of(c * chunk, chunk), chunk)

    in_q.wait()
    in_k.wait()
    in_v.wait()
    in_o.wait()

    def project(c):
        tok = tokens[row_slice(c), :].astype(F32)
        scaled = (tok * small[0:1, 0:feats]).astype(BF16)
        squares = jnp.sum(tok * tok, axis=1, keepdims=True)
        blocks = pl.ds(c * per_chunk, per_chunk)
        lanes = lax.broadcasted_iota(jnp.int32, (chunk, 128), 1)
        gates = lax.dot_general(
            scaled, w_gates[...], (((1,), (1,)), ((), ())), preferred_element_type=F32
        ) + jnp.where(lanes == 2 * heads, squares, 0.0)
        gate_send[blocks] = gates.reshape(per_chunk, seqs, 128)
        offset = 0
        for weight in (wq, wk, wv, wo):
            width = weight.shape[1]
            part = dot(scaled, weight[...]).reshape(per_chunk, seqs, width)
            proj_send[blocks, :, offset : offset + width] = part.astype(BF16)
            offset += width

    each(chunks, project)
    pl.semaphore_wait(barrier, n + tn - 2)

    def proj_copy(k):
        t = lax.rem(me + k, n)
        return ep_copy(0, k, proj_send.at[t], proj_recv.at[k - 1])

    def gate_copy(k):
        t = lax.rem(me + k, n)
        return ep_copy(1, k, gate_send.at[t], gate_recv.at[k - 1])

    peers(lambda k: (gate_copy(k).start(), proj_copy(k).start()))

    proj_acc = num
    gate_total = gate_send[me]
    proj_acc[...] = proj_send[me].astype(F32)
    if n <= 8:
        for k in range(1, n):
            gate_copy(k).wait_recv()
            gate_total = gate_total + gate_recv[k - 1]
    else:
        peers(lambda k: gate_copy(k).wait_recv())
        gate_total = lax.fori_loop(1, n, lambda k, acc: acc + gate_recv[k - 1], gate_total)

    def take_proj(k):
        proj_copy(k).wait_recv()
        proj_acc[...] += proj_recv[k - 1].astype(F32)

    inverse = lax.rsqrt(pick_lane(gate_total, 2 * heads) / d_model + EPSILON)
    gate_total = gate_total * inverse
    in_log = SOFT_CAP * jnp.tanh((gate_total + small[4:5, 0:128]) / SOFT_CAP)
    forget_pre = pltpu.roll(gate_total, 128 - heads, 1)
    capped = SOFT_CAP * jnp.tanh((forget_pre + small[5:6, 0:128]) / SOFT_CAP)
    forget_log = jnp.minimum(capped, 0.0) - jnp.log1p(jnp.exp(-jnp.abs(capped)))
    square[...] = jnp.zeros_like(square)
    square[0:heads, 0:seqs] = state_max[...]
    moved = forget_log + square[...].T[0:seqs, :]
    top = jnp.maximum(moved, in_log)
    carried = jnp.exp(moved - top)
    fresh = jnp.exp(in_log - top)
    floor = jnp.exp(-top)
    top_square = jnp.concatenate([top, jnp.zeros((128 - seqs, 128), F32)], axis=0).T
    new_max[...] = top_square[0:heads, 0:seqs]
    head_lane = lax.broadcasted_iota(jnp.int32, (seqs, hk), 1) // dk
    carried_cols = [pick_lane(carried, h) for h in range(heads)]
    floor_cols = [pick_lane(floor, h) for h in range(heads)]
    carried_wide = jnp.zeros((seqs, hk), F32)
    fresh_wide = jnp.zeros((seqs, hk), F32)
    for h in range(heads):
        carried_wide = jnp.where(head_lane == h, carried_cols[h], carried_wide)
        fresh_wide = jnp.where(head_lane == h, pick_lane(fresh, h), fresh_wide)

    peers(take_proj)

    def rounded(lo, width):
        return (proj_acc[:, lo : lo + width] * inverse).astype(BF16).astype(F32)

    query = rounded(0, hk) * dk ** (-0.5)
    key = rounded(hk, hk) * fresh_wide
    value = rounded(2 * hk, hv)
    outgate = rounded(2 * hk + hv, hv)
    for h in range(heads):
        norm_wide[:, h * dk : (h + 1) * dk] = state_norm[:, h, :]
    norm = carried_wide * norm_wide[...] + key
    new_norm[...] = norm
    product = norm * query
    padding = jnp.zeros((128 - seqs, hk), F32)
    query_t = jnp.concatenate([query, padding], axis=0).T
    key_t = jnp.concatenate([key, padding], axis=0).T
    in_s.wait()
    for h in range(heads):
        hs = slice(h * dk, (h + 1) * dk)
        readouts = []
        for r in range(seqs):
            state = (
                carried_cols[h][r : r + 1, :] * sm[r, h]
                + key_t[hs, r : r + 1] * value[r : r + 1, h * dv : (h + 1) * dv]
            )
            sm[r, h] = state
            readouts.append(jnp.sum(state * query_t[hs, r : r + 1], axis=0, keepdims=True))
        numerator = jnp.concatenate(readouts, axis=0)
        denominator = jnp.sum(jnp.where(head_lane == h, product, 0.0), axis=1, keepdims=True)
        readout = numerator / jnp.maximum(jnp.abs(denominator), floor_cols[h])
        cols = slice(h * dv, (h + 1) * dv)
        scale = lax.rsqrt(jnp.mean(readout * readout, axis=1, keepdims=True) + EPSILON)
        gated = readout * scale * small[3:4, cols]
        gated = gated * jax.nn.sigmoid(outgate[:, cols])
        heads_all[me, :, cols] = gated.astype(BF16)

    def heads_copy(k):
        return ep_copy(2, k, heads_all.at[me], heads_all.at[me])

    peers(lambda k: heads_copy(k).start())
    state_out = pltpu.make_async_copy(sm, new_matrix, local_sem.at[11])
    state_out.start()

    in_m.wait()
    peers(lambda k: heads_copy(k).wait_recv())

    def mix_rows(c):
        held = heads_all[pl.ds(c * per_chunk, per_chunk)].reshape(chunk, hv)
        mix_send[row_slice(c), :] = dot(held, wm[...]).astype(BF16)

    each(chunks, mix_rows)

    def quarter_of(t):
        return pl.ds(pl.multiple_of(t * quarter, quarter), quarter)

    def mix_copy(k):
        return tp_copy(
            0, k, mix_send.at[quarter_of(lax.rem(mt + k, tn)), :], mix_recv.at[k - 1]
        )

    tp_peers(lambda k: mix_copy(k).start())
    mine = quarter_of(mt)
    near = mt + 1 - 2 * lax.rem(mt, 2)
    far = lax.rem(mt + 2, tn)
    both = lax.rem(near + 2, tn)
    mixed = mix_send[mine, :].astype(F32)
    for k in range(1, tn):
        mix_copy(k).wait_recv()
        mixed = mixed + mix_recv[k - 1].astype(F32)
    hidden = (tokens[mine, :].astype(F32) + mixed.astype(BF16).astype(F32)).astype(BF16)
    held = hidden.astype(F32)
    hid_own[...] = held
    gained = held * small[1:2, 0:feats]
    y_all[me, mine, :] = gained.astype(BF16)
    squares = jnp.sum(held * held, axis=1, keepdims=True)
    gate_dot = jnp.sum(gained * small[2:3, 0:feats], axis=1, keepdims=True)
    piece = min(quarter, 128)
    pieces = quarter // piece
    lanes = lax.broadcasted_iota(jnp.int32, (quarter, 128), 1)
    stats = jnp.where(lanes == 0, squares, jnp.where(lanes == 1, gate_dot, 0.0))
    for j in range(pieces):
        block = stats[j * piece : (j + 1) * piece, :]
        if piece < 128:
            block = jnp.concatenate([block, jnp.zeros((128 - piece, 128), F32)], axis=0)
        stat_send[j] = block.T[0:8, :]

    def part_copy(partner, sems, k, src, dst):
        return pltpu.make_async_remote_copy(
            src_ref=src,
            dst_ref=dst,
            send_sem=pair_send.at[sems, k],
            recv_sem=pair_recv.at[sems, k],
            device_id={"tp": partner},
            device_id_type=MESH,
        )

    def source_of(k):
        return lax.rem(me + n - k, n)

    def target_of(k):
        return lax.rem(me + k, n)

    def y_copy(k):
        return ep_copy(3, k, y_all.at[me, mine, :], y_all.at[me, mine, :])

    def spread(partner, sems, k, rows_at):
        view = y_all.at[source_of(k), quarter_of(rows_at), :]
        return part_copy(partner, sems, k, view, view)

    def y_far(k):
        return spread(far, 0, k, mt)

    def y_near(k):
        return spread(near, 1, k, mt)

    def y_near_far(k):
        return spread(near, 2, k, far)

    def stat_copy(k):
        return ep_copy(4, k, stat_send, stat_recv.at[k - 1])

    def stat_tp(k):
        return tp_copy(1, k, stat_all.at[mt], stat_all.at[mt])

    def dense_copy(k):
        return ep_copy(5, k, dense_send.at[target_of(k)], dense_recv.at[k - 1])

    y_far(0).start()
    peers(lambda k: (stat_copy(k).start(), y_copy(k).start()))
    y_near(0).start()
    y_far(0).wait_recv()
    y_near_far(0).start()
    in_dg.wait()
    in_du.wait()
    y_near(0).wait_recv()
    y_near_far(0).wait_recv()

    def dense_rows(c):
        held = y_all[me, row_slice(c), :]
        blocks = pl.ds(c * per_chunk, per_chunk)
        for lo, weight in ((0, wdg), (units, wdu)):
            part = dot(held, weight[...]).reshape(per_chunk, seqs, units)
            dense_send[blocks, :, lo : lo + units] = part.astype(BF16)

    each(chunks, dense_rows)
    peers(lambda k: dense_copy(k).start())

    if n <= 8:
        stat_total = stat_send[...]
        for k in range(1, n):
            stat_copy(k).wait_recv()
            stat_total = stat_total + stat_recv[k - 1]
    else:
        peers(lambda k: stat_copy(k).wait_recv())
        stat_total = lax.fori_loop(1, n, lambda k, acc: acc + stat_recv[k - 1], stat_send[...])
    stat_all[mt] = stat_total
    tp_peers(lambda k: stat_tp(k).start())

    in_eg.wait()
    in_eu.wait()

    def expert_block(source, first):
        feat_rows = pl.ds(pl.multiple_of(source * feats, feats), feats)

        def body(c):
            held = y_all[source, row_slice(c), :]
            for lo, weight in ((0, weg), (units, weu)):
                cols = slice(lo, lo + units)
                part = dot(held, weight[feat_rows, :])
                if first:
                    exp_acc[row_slice(c), cols] = part
                else:
                    exp_acc[row_slice(c), cols] += part

        each(chunks, body)

    def forward(k):
        y_copy(k).wait_recv()
        y_far(k).start()
        y_near(k).start()

    def forward_far(k):
        y_far(k).wait_recv()
        y_near_far(k).start()

    def expert_step(k):
        y_near(k).wait_recv()
        y_near_far(k).wait_recv()
        expert_block(source_of(k), False)

    def staged(stages, least):
        if n <= 8:
            for i in range(least, n + len(stages) - 1):
                for late, stage in enumerate(stages):
                    if least <= i - late < n:
                        stage(i - late)
        else:
            for stage in stages:
                each(n - least, lambda i, stage=stage: stage(i + least))

    expert_block(me, True)
    staged((forward, forward_far, expert_step), 1)

    tp_peers(lambda k: stat_tp(k).wait_recv())
    for q in range(tn):
        for j in range(pieces):
            total = stat_all[q, j]
            columns = jnp.concatenate([total, jnp.zeros((120, 128), F32)], axis=0).T
            scale = lax.rsqrt(pick_lane(columns, 0) / d_model + EPSILON)
            at = q * quarter + j * piece
            inv_two[at : at + piece, :] = jnp.broadcast_to(scale, (128, 128))[0:piece]

    dense_total = dense_send[me].astype(F32)
    if n <= 8:
        for k in range(1, n):
            dense_copy(k).wait_recv()
            dense_total = dense_total + dense_recv[k - 1].astype(F32)
    else:
        peers(lambda k: dense_copy(k).wait_recv())
        dense_total = lax.fori_loop(
            1, n, lambda k, acc: acc + dense_recv[k - 1].astype(F32), dense_total
        )
    seq_scale = inv_two[pl.ds(pl.multiple_of(me * seqs, seqs), seqs), 0:1]
    dense_total = dense_total * seq_scale
    unit_all[me] = (
        jax.nn.silu(dense_total[:, 0:units]) * dense_total[:, units : 2 * units]
    ).astype(BF16)

    def unit_copy(k):
        return ep_copy(6, k, unit_all.at[me], unit_all.at[me])

    peers(lambda k: unit_copy(k).start())

    def expert_units(c):
        picks = routes[:, row_slice(c)] == me
        weight = jnp.sum(
            jnp.where(picks, route_weights[:, row_slice(c)], 0.0), axis=0, keepdims=True
        )
        weight = pick_lane(jnp.broadcast_to(weight, (chunk, chunk)).T, 0)
        scale = inv_two[row_slice(c), 0:1]
        gate = exp_acc[row_slice(c), 0:units] * scale
        up = exp_acc[row_slice(c), units : 2 * units] * scale
        exp_acc[row_slice(c), 0:units] = jax.nn.silu(gate) * up * weight

    each(chunks, expert_units)
    peers(lambda k: y_copy(k).wait_send())
    each(n, lambda k: (y_far(k).wait_send(), y_near(k).wait_send()))
    each(n, lambda k: y_near_far(k).wait_send())

    def result_view(k, rows_at):
        return y_all.at[target_of(k), quarter_of(rows_at), :]

    def res_near(k):
        return part_copy(near, 3, k, result_view(k, near), near_recv.at[k, 0])

    def res_near_far(k):
        return part_copy(near, 4, k, result_view(k, both), near_recv.at[k, 1])

    def res_far(k):
        return part_copy(far, 5, k, result_view(k, far), far_recv.at[k])

    def res_copy(k):
        return ep_copy(7, k, result_view(k, mt), res_recv.at[k - 1])

    def result_step(k):
        t = target_of(k)
        down_copy(t).wait()

        def body(c):
            held = exp_acc[row_slice(c), 0:units].astype(BF16)
            y_all[t, row_slice(c), :] = dot(held, wed[t]).astype(BF16)

        each(chunks, body)
        res_near_far(k).start()
        res_near(k).start()

    def result_far(k):
        res_near_far(k).wait_recv()
        summed = y_all[target_of(k), quarter_of(far), :].astype(F32) + near_recv[k, 1].astype(F32)
        y_all[target_of(k), quarter_of(far), :] = summed.astype(BF16)
        res_far(k).start()

    def result_sum(k):
        res_near(k).wait_recv()
        res_far(k).wait_recv()
        return (
            y_all[target_of(k), mine, :].astype(F32)
            + near_recv[k, 0].astype(F32)
            + far_recv[k].astype(F32)
        )

    def result_out(k):
        y_all[target_of(k), mine, :] = result_sum(k).astype(BF16)
        res_copy(k).start()

    staged((result_step, result_far, result_out), 1)

    result_step(0)
    in_dd.wait()
    peers(lambda k: unit_copy(k).wait_recv())

    def down_rows(c):
        hidden_units = unit_all[pl.ds(c * per_chunk, per_chunk)].reshape(chunk, units)
        fin_send[row_slice(c), :] = dot(hidden_units, wdd[...]).astype(BF16)

    each(chunks, down_rows)

    def fin_copy(k):
        return tp_copy(
            2, k, fin_send.at[quarter_of(lax.rem(mt + k, tn)), :], fin_recv.at[k - 1]
        )

    tp_peers(lambda k: fin_copy(k).start())
    result_far(0)
    dense = fin_send[mine, :].astype(F32)
    for k in range(1, tn):
        fin_copy(k).wait_recv()
        dense = dense + fin_recv[k - 1].astype(F32)
    gates = []
    for j in range(pieces):
        columns = jnp.concatenate([stat_total[j], jnp.zeros((120, 128), F32)], axis=0).T
        scale = lax.rsqrt(pick_lane(columns, 0) / d_model + EPSILON)
        gates.append(jax.nn.sigmoid(scale * pick_lane(columns, 1))[0:piece])
    gate = gates[0] if pieces == 1 else jnp.concatenate(gates, axis=0)
    out_acc[...] = result_sum(0) + gate * dense

    def take_result(k):
        res_copy(k).wait_recv()
        out_acc[...] += res_recv[k - 1].astype(F32)

    peers(take_result)
    fin_all[mine, :] = (hid_own[...] + out_acc[...]).astype(BF16)

    def all_copy(k):
        return tp_copy(3, k, fin_all.at[mine, :], fin_all.at[mine, :])

    tp_peers(lambda k: all_copy(k).start())
    tp_peers(lambda k: all_copy(k).wait_recv())
    layer_out[...] = fin_all[...]
    state_out.wait()
    for copies in (
        proj_copy,
        gate_copy,
        heads_copy,
        stat_copy,
        dense_copy,
        unit_copy,
        res_copy,
    ):
        peers(lambda k, copies=copies: copies(k).wait_send())
    for copies in (res_near, res_near_far, res_far):
        each(n, lambda k, copies=copies: copies(k).wait_send())
    for copies in (mix_copy, stat_tp, fin_copy, all_copy):
        tp_peers(lambda k, copies=copies: copies(k).wait_send())


def on_device(
    n,
    tn,
    tokens,
    mix_gain,
    w_query,
    w_key,
    w_value,
    w_outgate,
    w_igate,
    w_fgate,
    igate_bias,
    fgate_bias,
    head_gain,
    w_mixout,
    state_matrix,
    state_norm,
    state_max,
    ffn_gain,
    dense_mix,
    w_dense_gate,
    w_dense_up,
    w_dense_down,
    routes,
    route_weights,
    w_exp_gate,
    w_exp_up,
    w_exp_down,
):
    rows, feats = tokens.shape
    seqs, heads, dk, dv = state_matrix.shape
    hk, hv = heads * dk, heads * dv
    units = w_dense_gate.shape[1]
    wide = 2 * hk + 2 * hv
    quarter = rows // tn
    pieces = max(1, quarter // 128)
    w_gates = jnp.pad(
        jnp.concatenate([w_igate.T, w_fgate.T], axis=0), ((0, 128 - 2 * heads), (0, 0))
    )
    width = max(feats, hv, 128)
    row_at = lax.broadcasted_iota(jnp.int32, (8, width), 0)
    small = jnp.zeros((8, width), F32)
    for at, row in enumerate(
        (mix_gain, ffn_gain, dense_mix, head_gain, igate_bias, fgate_bias)
    ):
        wide_row = jnp.pad(row.astype(F32), (0, width - row.shape[0]))
        small = jnp.where(row_at == at, wide_row[None, :], small)
    down = w_exp_down
    if feats % 128:
        down = w_exp_down[0].reshape(units, n, feats).transpose(1, 0, 2)
    vmem = pl.BlockSpec(memory_space=pltpu.VMEM)
    hbm = pl.BlockSpec(memory_space=pl.ANY)
    dma = pltpu.SemaphoreType.DMA
    scratch = [
        pltpu.VMEM(w_query.shape, BF16),
        pltpu.VMEM(w_key.shape, BF16),
        pltpu.VMEM(w_value.shape, BF16),
        pltpu.VMEM(w_outgate.shape, BF16),
        pltpu.VMEM(w_mixout.shape, BF16),
        pltpu.VMEM(state_matrix.shape, F32),
        pltpu.VMEM(w_dense_gate.shape, BF16),
        pltpu.VMEM(w_dense_up.shape, BF16),
        pltpu.VMEM(w_dense_down.shape, BF16),
        pltpu.VMEM(w_exp_gate.shape[1:], BF16),
        pltpu.VMEM(w_exp_up.shape[1:], BF16),
        pltpu.VMEM((n, units, feats), BF16),
        pltpu.VMEM((n, seqs, wide), BF16),
        pltpu.VMEM((n - 1, seqs, wide), BF16),
        pltpu.VMEM((n, seqs, 128), F32),
        pltpu.VMEM((n - 1, seqs, 128), F32),
        pltpu.VMEM((seqs, wide), F32),
        pltpu.VMEM((n, seqs, hv), BF16),
        pltpu.VMEM((rows, feats), BF16),
        pltpu.VMEM((tn - 1, quarter, feats), BF16),
        pltpu.VMEM((quarter, feats), F32),
        pltpu.VMEM((n, rows, feats), BF16),
        pltpu.VMEM((pieces, 8, 128), F32),
        pltpu.VMEM((n - 1, pieces, 8, 128), F32),
        pltpu.VMEM((tn, pieces, 8, 128), F32),
        pltpu.VMEM((rows, 128), F32),
        pltpu.VMEM((n, seqs, 2 * units), BF16),
        pltpu.VMEM((n - 1, seqs, 2 * units), BF16),
        pltpu.VMEM((n, seqs, units), BF16),
        pltpu.VMEM((rows, 2 * units), F32),
        pltpu.VMEM((n, 2, quarter, feats), BF16),
        pltpu.VMEM((n, quarter, feats), BF16),
        pltpu.VMEM((n - 1, quarter, feats), BF16),
        pltpu.VMEM((quarter, feats), F32),
        pltpu.VMEM((rows, feats), BF16),
        pltpu.VMEM((tn - 1, quarter, feats), BF16),
        pltpu.VMEM((rows, feats), BF16),
        pltpu.VMEM((seqs, hk), F32),
        pltpu.VMEM((128, 128), F32),
        dma((12,)),
        dma((n,)),
        dma((8, n - 1)),
        dma((8, n - 1)),
        dma((4, tn - 1)),
        dma((4, tn - 1)),
        dma((6, n)),
        dma((6, n)),
    ]
    layer_out, new_matrix, new_norm, new_max = pl.pallas_call(
        functools.partial(layer_kernel, n, tn, n * feats),
        out_shape=(
            jax.ShapeDtypeStruct((rows, feats), BF16),
            jax.ShapeDtypeStruct(state_matrix.shape, F32),
            jax.ShapeDtypeStruct((seqs, hk), F32),
            jax.ShapeDtypeStruct((heads, seqs), F32),
        ),
        in_specs=[vmem] * 7 + [hbm] * 12,
        out_specs=(vmem, hbm, vmem, vmem),
        scratch_shapes=scratch,
        compiler_params=pltpu.CompilerParams(
            collective_id=0, has_side_effects=True, vmem_limit_bytes=66_900_000
        ),
    )(
        tokens,
        small,
        w_gates,
        state_norm,
        state_max.T,
        routes.T,
        route_weights.T,
        w_query,
        w_key,
        w_value,
        w_outgate,
        w_mixout,
        state_matrix,
        w_dense_gate,
        w_dense_up,
        w_dense_down,
        w_exp_gate,
        w_exp_up,
        down,
    )
    return (
        layer_out,
        new_matrix,
        new_norm.reshape(seqs, heads, dk),
        new_max.T,
    )


def solution(mesh):
    return jax.shard_map(
        functools.partial(on_device, mesh.shape["ep"], mesh.shape["tp"]),
        mesh=mesh,
        in_specs=(
            P(None, "ep"),
            P("ep"),
            P("ep", "tp"),
            P("ep", "tp"),
            P("ep", "tp"),
            P("ep", "tp"),
            P("ep", "tp"),
            P("ep", "tp"),
            P("tp"),
            P("tp"),
            P("tp"),
            P("tp", "ep"),
            P("ep", "tp", None, None),
            P("ep", "tp", None),
            P("ep", "tp"),
            P("ep"),
            P("ep"),
            P("ep", "tp"),
            P("ep", "tp"),
            P("tp", "ep"),
            P(),
            P(),
            P("ep", None, "tp"),
            P("ep", None, "tp"),
            P("ep", "tp", None),
        ),
        out_specs=(P(None, "ep"), P("ep", "tp", None, None), P("ep", "tp", None), P("ep", "tp")),
        check_vma=False,
    )
```

profile of v0, /device:TPU:29, one launch (start us, length us, event | category | flops | bytes accessed | tf_op | source)
XLA Modules:
  0.0 87.1 jit_solution(8971754964892300071)
XLA Ops:
  0.7 0.7 convert_element_type.17
  1.4 0.7 convert_element_type.18
  2.0 0.7 convert_element_type.19
  2.7 0.7 convert_element_type.20
  3.4 0.7 pad.11
  4.1 0.7 pad.12
  4.7 0.7 select_select_fusion.small
  5.4 1.4 %fusion.2.w_gates = bf16[128,512]{1,0:T(8,128)(2,1)} fusion(bf16[4,512]{1,0:T(4,128)(2,1)} %bitcast.6, bf16[4,512]{1,0:T(4,128)(2,1)} %bitcast.7), kind=kLoop, calls=%fused_computation.3 | loop fusion | flops 458752 | bytes 139264 | tf_op jit(solution)/shard_map/concatenate | solution.py:659
  6.8 73.6 %shard_map.264 = (bf16[128,512]{1,0:T(8,128)(2,1)}, f32[16,4,64,128]{3,2,1,0:T(8,128)}, f32[16,256]{1,0:T(8,128)}, f32[4,16]{1,0:T(4,128)}) custom-call(bf16[128,512]{1,0:T(8,128)(2,1)} %tokens.1, f32[8,512]{1,0:T(8,128)} %select_select_fusion.small, bf16[128,512]{1,0:T(8,128)(2,1)} %fusion.2.w_gates, f32[16,4,64]{2,1,0:T(4,128)} %state_norm.1, ...), custom_call_target="tpu_custom_call" | custom-call | tf_op jit(solution)/shard_map/pallas_call | solution.py:724
  80.4 1.4 %reshape.17 = f32[16,4,64]{2,1,0:T(4,128)} reshape(f32[16,256]{1,0:T(8,128)} %get-tuple-element.10) | data formatting | bytes 32768 | tf_op jit(solution)/shard_map/reshape | solution.py:762
  81.8 1.6 %copy.32 = bf16[128,512]{1,0:T(8,128)(2,1)} copy(bf16[128,512]{1,0:T(8,128)(2,1)} %get-tuple-element.22) | data formatting | bytes 262144
  83.4 0.0 copy-start
  83.4 3.2 %copy.33 = f32[16,4,64,128]{3,2,1,0:T(8,128)} copy(f32[16,4,64,128]{3,2,1,0:T(8,128)} %get-tuple-element.23) | data formatting | bytes 4194304
  86.6 0.0 copy-done
  86.6 0.6 copy.34
  (3 shorter events, 0.0 us)
Async XLA Ops:
  83.4 3.2 %copy-start = (f32[4,16]{1,0:T(4,128)S(1)}, f32[4,16]{1,0:T(4,128)}, u32[]{:S(2)}) copy-start(f32[4,16]{1,0:T(4,128)} %get-tuple-element.11) | copy-start | bytes 772
where the time goes:
time: 87.5 us; the launch traced here: 87.1 us
  Pallas kernels  73.6 us (84%)
  local copies, waits for them, and re-layouts  8.04 us (9%)
  other arithmetic  4.79 us (5%)
    pallas_call x1, Pallas kernels, on_device(): pl.pallas_call(functools.partial(layer_kernel, n, tn, n * feats), out_sha...  73.6 us
    unnamed x5, local copies, waits for them, and re-layouts  5.31 us
    convert_element_type x4, other arithmetic, on_device(): wide_row = jnp.pad(row.astype(F32), (0, width - row.shape[0]))  2.73 us

commit v1 on v0

--- a/solution.py
+++ b/solution.py
@@ -35,6 +35,852 @@
 
 
 def layer_kernel(
+    n,
+    tn,
+    d_model,
+    tokens_in,
+    mix_gain_in,
+    w_query,
+    w_key,
+    w_value,
+    w_outgate,
+    w_igate_in,
+    w_fgate_in,
+    igate_bias_in,
+    fgate_bias_in,
+    head_gain_in,
+    w_mixout,
+    state_matrix,
+    state_norm_in,
+    state_max_in,
+    ffn_gain_in,
+    dense_mix_in,
+    w_dense_gate,
+    w_dense_up,
+    w_dense_down,
+    routes_in,
+    route_weights_in,
+    w_exp_gate,
+    w_exp_up,
+    w_exp_down,
+    layer_out,
+    new_matrix,
+    new_norm,
+    new_max,
+    tokens,
+    mix_gain_v,
+    w_igate,
+    w_fgate,
+    igate_bias,
+    fgate_bias,
+    head_gain_v,
+    state_norm,
+    state_max,
+    ffn_gain_v,
+    dense_mix_v,
+    routes,
+    route_weights,
+    norm_out,
+    max_out,
+    wq,
+    wk,
+    wv,
+    wo,
+    wm,
+    sm,
+    wdg,
+    wdu,
+    wdd,
+    weg,
+    weu,
+    wed,
+    proj_send,
+    proj_recv,
+    gate_send,
+    gate_recv,
+    num,
+    heads_all,
+    mix_send,
+    mix_recv,
+    hid_own,
+    y_all,
+    stat_send,
+    stat_recv,
+    stat_all,
+    inv_two,
+    dense_send,
+    dense_recv,
+    unit_all,
+    exp_acc,
+    near_recv,
+    far_recv,
+    res_recv,
+    out_acc,
+    fin_send,
+    fin_recv,
+    fin_all,
+    norm_wide,
+    square,
+    input_sem,
+    local_sem,
+    down_sem,
+    ep_send,
+    ep_recv,
+    tp_send,
+    tp_recv,
+    pair_send,
+    pair_recv,
+):
+    me = lax.axis_index("ep")
+    mt = lax.axis_index("tp")
+    rows, feats = tokens_in.shape
+    chunk = min(rows, 128)
+    chunks = rows // chunk
+    seqs = state_norm_in.shape[0]
+    heads, dk, dv = sm.shape[1], sm.shape[2], sm.shape[3]
+    hk, hv = heads * dk, heads * dv
+    units = wdg.shape[1]
+    quarter = rows // tn
+    per_chunk = chunk // seqs
+
+    def fetch(i, src, dst):
+        copy = pltpu.make_async_copy(src, dst, local_sem.at[i])
+        copy.start()
+        return copy
+
+    def fetch_input(i, src, dst):
+        copy = pltpu.make_async_copy(src, dst, input_sem.at[i])
+        copy.start()
+        return copy
+
+    first_inputs = [
+        fetch_input(i, src, dst)
+        for i, (src, dst) in enumerate(
+            (
+                (tokens_in, tokens),
+                (mix_gain_in, mix_gain_v),
+                (w_igate_in, w_igate),
+                (w_fgate_in, w_fgate),
+            )
+        )
+    ]
+    in_q = fetch(0, w_query, wq)
+    in_k = fetch(1, w_key, wk)
+    in_v = fetch(2, w_value, wv)
+    in_o = fetch(3, w_outgate, wo)
+    in_s = fetch(4, state_matrix, sm)
+    later_inputs = [
+        fetch_input(4 + i, src, dst)
+        for i, (src, dst) in enumerate(
+            (
+                (igate_bias_in, igate_bias),
+                (fgate_bias_in, fgate_bias),
+                (head_gain_in, head_gain_v),
+                (state_norm_in, state_norm),
+                (state_max_in, state_max),
+                (ffn_gain_in, ffn_gain_v),
+                (dense_mix_in, dense_mix_v),
+                (routes_in, routes),
+                (route_weights_in, route_weights),
+            )
+        )
+    ]
+    in_m = fetch(5, w_mixout, wm)
+    in_dg = fetch(6, w_dense_gate, wdg)
+    in_du = fetch(7, w_dense_up, wdu)
+    in_dd = fetch(8, w_dense_down, wdd)
+    in_eg = fetch(9, w_exp_gate.at[0], weg)
+    in_eu = fetch(10, w_exp_up.at[0], weu)
+
+    def down_copy(t):
+        if w_exp_down.shape[2] == n * feats:
+            src = w_exp_down.at[0, :, pl.ds(pl.multiple_of(t * feats, 128), feats)]
+        else:
+            src = w_exp_down.at[t]
+        return pltpu.make_async_copy(src, wed.at[t], down_sem.at[t])
+
+    each(n, lambda t: down_copy(t).start())
+
+    def ep_copy(phase, k, src, dst):
+        return pltpu.make_async_remote_copy(
+            src_ref=src,
+            dst_ref=dst,
+            send_sem=ep_send.at[phase, k - 1],
+            recv_sem=ep_recv.at[phase, k - 1],
+            device_id={"ep": lax.rem(me + k, n)},
+            device_id_type=MESH,
+        )
+
+    def tp_copy(phase, k, src, dst):
+        return pltpu.make_async_remote_copy(
+            src_ref=src,
+            dst_ref=dst,
+            send_sem=tp_send.at[phase, k - 1],
+            recv_sem=tp_recv.at[phase, k - 1],
+            device_id={"tp": lax.rem(mt + k, tn)},
+            device_id_type=MESH,
+        )
+
+    def peers(body):
+        each(n - 1, lambda i: body(i + 1))
+
+    def tp_peers(body):
+        each(tn - 1, lambda i: body(i + 1))
+
+    barrier = pltpu.get_barrier_semaphore()
+    peers(
+        lambda k: pl.semaphore_signal(
+            barrier, inc=1, device_id={"ep": lax.rem(me + k, n)}, device_id_type=MESH
+        )
+    )
+    tp_peers(
+        lambda k: pl.semaphore_signal(
+            barrier, inc=1, device_id={"tp": lax.rem(mt + k, tn)}, device_id_type=MESH
+        )
+    )
+
+    def row_slice(c):
+        return pl.ds(pl.multiple_of(c * chunk, chunk), chunk)
+
+    for copy in first_inputs:
+        copy.wait()
+    mix_gain = mix_gain_v[...].astype(F32).reshape(1, feats)
+    gate_weights = jnp.concatenate(
+        [w_igate[...].astype(F32), w_fgate[...].astype(F32), jnp.zeros((128 - 2 * heads, feats), F32)],
+        axis=0,
+    ).astype(BF16)
+    in_q.wait()
+    in_k.wait()
+    in_v.wait()
+    in_o.wait()
+
+    def project(c):
+        tok = tokens[row_slice(c), :].astype(F32)
+        scaled = (tok * mix_gain).astype(BF16)
+        squares = jnp.sum(tok * tok, axis=1, keepdims=True)
+        blocks = pl.ds(c * per_chunk, per_chunk)
+        lanes = lax.broadcasted_iota(jnp.int32, (chunk, 128), 1)
+        gates = lax.dot_general(
+            scaled, gate_weights, (((1,), (1,)), ((), ())), preferred_element_type=F32
+        ) + jnp.where(lanes == 2 * heads, squares, 0.0)
+        gate_send[blocks] = gates.reshape(per_chunk, seqs, 128)
+        offset = 0
+        for weight in (wq, wk, wv, wo):
+            width = weight.shape[1]
+            part = dot(scaled, weight[...]).reshape(per_chunk, seqs, width)
+            proj_send[blocks, :, offset : offset + width] = part.astype(BF16)
+            offset += width
+
+    each(chunks, project)
+    pl.semaphore_wait(barrier, n + tn - 2)
+
+    def proj_copy(k):
+        t = lax.rem(me + k, n)
+        return ep_copy(0, k, proj_send.at[t], proj_recv.at[k - 1])
+
+    def gate_copy(k):
+        t = lax.rem(me + k, n)
+        return ep_copy(1, k, gate_send.at[t], gate_recv.at[k - 1])
+
+    peers(lambda k: (gate_copy(k).start(), proj_copy(k).start()))
+
+    proj_acc = num
+    gate_total = gate_send[me]
+    proj_acc[...] = proj_send[me].astype(F32)
+    if n <= 8:
+        for k in range(1, n):
+            gate_copy(k).wait_recv()
+            gate_total = gate_total + gate_recv[k - 1]
+    else:
+        peers(lambda k: gate_copy(k).wait_recv())
+        gate_total = lax.fori_loop(1, n, lambda k, acc: acc + gate_recv[k - 1], gate_total)
+
+    def take_proj(k):
+        proj_copy(k).wait_recv()
+        proj_acc[...] += proj_recv[k - 1].astype(F32)
+
+    for copy in later_inputs:
+        copy.wait()
+    bias_lane = lax.broadcasted_iota(jnp.int32, (1, 128), 1)
+    in_bias = jnp.zeros((1, 128), F32)
+    forget_bias = jnp.zeros((1, 128), F32)
+    for h in range(heads):
+        in_bias = jnp.where(bias_lane == h, igate_bias[h], in_bias)
+        forget_bias = jnp.where(bias_lane == h, fgate_bias[h], forget_bias)
+    head_gain = head_gain_v[...].astype(F32).reshape(1, hv)
+    ffn_gain = ffn_gain_v[...].astype(F32).reshape(1, feats)
+    dense_mix = dense_mix_v[...].astype(F32).reshape(1, feats)
+
+    inverse = lax.rsqrt(pick_lane(gate_total, 2 * heads) / d_model + EPSILON)
+    gate_total = gate_total * inverse
+    in_log = SOFT_CAP * jnp.tanh((gate_total + in_bias) / SOFT_CAP)
+    forget_pre = pltpu.roll(gate_total, 128 - heads, 1)
+    capped = SOFT_CAP * jnp.tanh((forget_pre + forget_bias) / SOFT_CAP)
+    forget_log = jnp.minimum(capped, 0.0) - jnp.log1p(jnp.exp(-jnp.abs(capped)))
+    square[...] = jnp.zeros_like(square)
+    square[0:heads, 0:seqs] = state_max[...]
+    moved = forget_log + square[...].T[0:seqs, :]
+    top = jnp.maximum(moved, in_log)
+    carried = jnp.exp(moved - top)
+    fresh = jnp.exp(in_log - top)
+    floor = jnp.exp(-top)
+    top_square = jnp.concatenate([top, jnp.zeros((128 - seqs, 128), F32)], axis=0).T
+    max_out[...] = top_square[0:heads, 0:seqs]
+    max_copy = pltpu.make_async_copy(max_out, new_max, input_sem.at[13])
+    max_copy.start()
+    head_lane = lax.broadcasted_iota(jnp.int32, (seqs, hk), 1) // dk
+    carried_cols = [pick_lane(carried, h) for h in range(heads)]
+    floor_cols = [pick_lane(floor, h) for h in range(heads)]
+    carried_wide = jnp.zeros((seqs, hk), F32)
+    fresh_wide = jnp.zeros((seqs, hk), F32)
+    for h in range(heads):
+        carried_wide = jnp.where(head_lane == h, carried_cols[h], carried_wide)
+        fresh_wide = jnp.where(head_lane == h, pick_lane(fresh, h), fresh_wide)
+
+    peers(take_proj)
+
+    def rounded(lo, width):
+        return (proj_acc[:, lo : lo + width] * inverse).astype(BF16).astype(F32)
+
+    query = rounded(0, hk) * dk ** (-0.5)
+    key = rounded(hk, hk) * fresh_wide
+    value = rounded(2 * hk, hv)
+    outgate = rounded(2 * hk + hv, hv)
+    for h in range(heads):
+        norm_wide[:, h * dk : (h + 1) * dk] = state_norm[:, h, :]
+    norm = carried_wide * norm_wide[...] + key
+    for h in range(heads):
+        norm_out[:, h, :] = norm[:, h * dk : (h + 1) * dk]
+    norm_copy = pltpu.make_async_copy(norm_out, new_norm, input_sem.at[14])
+    norm_copy.start()
+    product = norm * query
+    padding = jnp.zeros((128 - seqs, hk), F32)
+    query_t = jnp.concatenate([query, padding], axis=0).T
+    key_t = jnp.concatenate([key, padding], axis=0).T
+    in_s.wait()
+    for h in range(heads):
+        hs = slice(h * dk, (h + 1) * dk)
+        readouts = []
+        for r in range(seqs):
+            state = (
+                carried_cols[h][r : r + 1, :] * sm[r, h]
+                + key_t[hs, r : r + 1] * value[r : r + 1, h * dv : (h + 1) * dv]
+            )
+            sm[r, h] = state
+            readouts.append(jnp.sum(state * query_t[hs, r : r + 1], axis=0, keepdims=True))
+        numerator = jnp.concatenate(readouts, axis=0)
+        denominator = jnp.sum(jnp.where(head_lane == h, product, 0.0), axis=1, keepdims=True)
+        readout = numerator / jnp.maximum(jnp.abs(denominator), floor_cols[h])
+        cols = slice(h * dv, (h + 1) * dv)
+        scale = lax.rsqrt(jnp.mean(readout * readout, axis=1, keepdims=True) + EPSILON)
+        gated = readout * scale * head_gain[:, cols]
+        gated = gated * jax.nn.sigmoid(outgate[:, cols])
+        heads_all[me, :, cols] = gated.astype(BF16)
+
+    def heads_copy(k):
+        return ep_copy(2, k, heads_all.at[me], heads_all.at[me])
+
+    peers(lambda k: heads_copy(k).start())
+    state_out = pltpu.make_async_copy(sm, new_matrix, local_sem.at[11])
+    state_out.start()
+
+    in_m.wait()
+    peers(lambda k: heads_copy(k).wait_recv())
+
+    def mix_rows(c):
+        held = heads_all[pl.ds(c * per_chunk, per_chunk)].reshape(chunk, hv)
+        mix_send[row_slice(c), :] = dot(held, wm[...]).astype(BF16)
+
+    each(chunks, mix_rows)
+
+    def quarter_of(t):
+        return pl.ds(pl.multiple_of(t * quarter, quarter), quarter)
+
+    def mix_copy(k):
+        return tp_copy(
+            0, k, mix_send.at[quarter_of(lax.rem(mt + k, tn)), :], mix_recv.at[k - 1]
+        )
+
+    tp_peers(lambda k: mix_copy(k).start())
+    mine = quarter_of(mt)
+    near = mt + 1 - 2 * lax.rem(mt, 2)
+    far = lax.rem(mt + 2, tn)
+    both = lax.rem(near + 2, tn)
+    mixed = mix_send[mine, :].astype(F32)
+    for k in range(1, tn):
+        mix_copy(k).wait_recv()
+        mixed = mixed + mix_recv[k - 1].astype(F32)
+    hidden = (tokens[mine, :].astype(F32) + mixed.astype(BF16).astype(F32)).astype(BF16)
+    held = hidden.astype(F32)
+    hid_own[...] = held
+    gained = held * ffn_gain
+    y_all[me, mine, :] = gained.astype(BF16)
+    squares = jnp.sum(held * held, axis=1, keepdims=True)
+    gate_dot = jnp.sum(gained * dense_mix, axis=1, keepdims=True)
+    piece = min(quarter, 128)
+    pieces = quarter // piece
+    lanes = lax.broadcasted_iota(jnp.int32, (quarter, 128), 1)
+    stats = jnp.where(lanes == 0, squares, jnp.where(lanes == 1, gate_dot, 0.0))
+    for j in range(pieces):
+        block = stats[j * piece : (j + 1) * piece, :]
+        if piece < 128:
+            block = jnp.concatenate([block, jnp.zeros((128 - piece, 128), F32)], axis=0)
+        stat_send[j] = block.T[0:8, :]
+
+    def part_copy(partner, sems, k, src, dst):
+        return pltpu.make_async_remote_copy(
+            src_ref=src,
+            dst_ref=dst,
+            send_sem=pair_send.at[sems, k],
+            recv_sem=pair_recv.at[sems, k],
+            device_id={"tp": partner},
+            device_id_type=MESH,
+        )
+
+    def source_of(k):
+        return lax.rem(me + n - k, n)
+
+    def target_of(k):
+        return lax.rem(me + k, n)
+
+    def y_copy(k):
+        return ep_copy(3, k, y_all.at[me, mine, :], y_all.at[me, mine, :])
+
+    def spread(partner, sems, k, rows_at):
+        view = y_all.at[source_of(k), quarter_of(rows_at), :]
+        return part_copy(partner, sems, k, view, view)
+
+    def y_far(k):
+        return spread(far, 0, k, mt)
+
+    def y_near(k):
+        return spread(near, 1, k, mt)
+
+    def y_near_far(k):
+        return spread(near, 2, k, far)
+
+    def stat_copy(k):
+        return ep_copy(4, k, stat_send, stat_recv.at[k - 1])
+
+    def stat_tp(k):
+        return tp_copy(1, k, stat_all.at[mt], stat_all.at[mt])
+
+    def dense_copy(k):
+        return ep_copy(5, k, dense_send.at[target_of(k)], dense_recv.at[k - 1])
+
+    y_far(0).start()
+    peers(lambda k: (stat_copy(k).start(), y_copy(k).start()))
+    y_near(0).start()
+    y_far(0).wait_recv()
+    y_near_far(0).start()
+    in_dg.wait()
+    in_du.wait()
+    y_near(0).wait_recv()
+    y_near_far(0).wait_recv()
+
+    def dense_rows(c):
+        held = y_all[me, row_slice(c), :]
+        blocks = pl.ds(c * per_chunk, per_chunk)
+        for lo, weight in ((0, wdg), (units, wdu)):
+            part = dot(held, weight[...]).reshape(per_chunk, seqs, units)
+            dense_send[blocks, :, lo : lo + units] = part.astype(BF16)
+
+    each(chunks, dense_rows)
+    peers(lambda k: dense_copy(k).start())
+
+    if n <= 8:
+        stat_total = stat_send[...]
+        for k in range(1, n):
+            stat_copy(k).wait_recv()
+            stat_total = stat_total + stat_recv[k - 1]
+    else:
+        peers(lambda k: stat_copy(k).wait_recv())
+        stat_total = lax.fori_loop(1, n, lambda k, acc: acc + stat_recv[k - 1], stat_send[...])
+    stat_all[mt] = stat_total
+    tp_peers(lambda k: stat_tp(k).start())
+
+    in_eg.wait()
+    in_eu.wait()
+
+    def expert_block(source, first):
+        feat_rows = pl.ds(pl.multiple_of(source * feats, feats), feats)
+
+        def body(c):
+            held = y_all[source, row_slice(c), :]
+            for lo, weight in ((0, weg), (units, weu)):
+                cols = slice(lo, lo + units)
+                part = dot(held, weight[feat_rows, :])
+                if first:
+                    exp_acc[row_slice(c), cols] = part
+                else:
+                    exp_acc[row_slice(c), cols] += part
+
+        each(chunks, body)
+
+    def forward(k):
+        y_copy(k).wait_recv()
+        y_far(k).start()
+        y_near(k).start()
+
+    def forward_far(k):
+        y_far(k).wait_recv()
+        y_near_far(k).start()
+
+    def expert_step(k):
+        y_near(k).wait_recv()
+        y_near_far(k).wait_recv()
+        expert_block(source_of(k), False)
+
+    def staged(stages, least):
+        if n <= 8:
+            for i in range(least, n + len(stages) - 1):
+                for late, stage in enumerate(stages):
+                    if least <= i - late < n:
+                        stage(i - late)
+        else:
+            for stage in stages:
+                each(n - least, lambda i, stage=stage: stage(i + least))
+
+    expert_block(me, True)
+    staged((forward, forward_far, expert_step), 1)
+
+    tp_peers(lambda k: stat_tp(k).wait_recv())
+    for q in range(tn):
+        for j in range(pieces):
+            total = stat_all[q, j]
+            columns = jnp.concatenate([total, jnp.zeros((120, 128), F32)], axis=0).T
+            scale = lax.rsqrt(pick_lane(columns, 0) / d_model + EPSILON)
+            at = q * quarter + j * piece
+            inv_two[at : at + piece, :] = jnp.broadcast_to(scale, (128, 128))[0:piece]
+
+    dense_total = dense_send[me].astype(F32)
+    if n <= 8:
+        for k in range(1, n):
+            dense_copy(k).wait_recv()
+            dense_total = dense_total + dense_recv[k - 1].astype(F32)
+    else:
+        peers(lambda k: dense_copy(k).wait_recv())
+        dense_total = lax.fori_loop(
+            1, n, lambda k, acc: acc + dense_recv[k - 1].astype(F32), dense_total
+        )
+    seq_scale = inv_two[pl.ds(pl.multiple_of(me * seqs, seqs), seqs), 0:1]
+    dense_total = dense_total * seq_scale
+    unit_all[me] = (
+        jax.nn.silu(dense_total[:, 0:units]) * dense_total[:, units : 2 * units]
+    ).astype(BF16)
+
+    def unit_copy(k):
+        return ep_copy(6, k, unit_all.at[me], unit_all.at[me])
+
+    peers(lambda k: unit_copy(k).start())
+
+    def expert_units(c):
+        picks = routes[:, row_slice(c)] == me
+        weight = jnp.sum(
+            jnp.where(picks, route_weights[:, row_slice(c)], 0.0), axis=0, keepdims=True
+        )
+        weight = pick_lane(jnp.broadcast_to(weight, (chunk, chunk)).T, 0)
+        scale = inv_two[row_slice(c), 0:1]
+        gate = exp_acc[row_slice(c), 0:units] * scale
+        up = exp_acc[row_slice(c), units : 2 * units] * scale
+        exp_acc[row_slice(c), 0:units] = jax.nn.silu(gate) * up * weight
+
+    each(chunks, expert_units)
+    peers(lambda k: y_copy(k).wait_send())
+    each(n, lambda k: (y_far(k).wait_send(), y_near(k).wait_send()))
+    each(n, lambda k: y_near_far(k).wait_send())
+
+    def result_view(k, rows_at):
+        return y_all.at[target_of(k), quarter_of(rows_at), :]
+
+    def res_near(k):
+        return part_copy(near, 3, k, result_view(k, near), near_recv.at[k, 0])
+
+    def res_near_far(k):
+        return part_copy(near, 4, k, result_view(k, both), near_recv.at[k, 1])
+
+    def res_far(k):
+        return part_copy(far, 5, k, result_view(k, far), far_recv.at[k])
+
+    def res_copy(k):
+        return ep_copy(7, k, result_view(k, mt), res_recv.at[k - 1])
+
+    def result_step(k):
+        t = target_of(k)
+        down_copy(t).wait()
+
+        def body(c):
+            held = exp_acc[row_slice(c), 0:units].astype(BF16)
+            y_all[t, row_slice(c), :] = dot(held, wed[t]).astype(BF16)
+
+        each(chunks, body)
+        res_near_far(k).start()
+        res_near(k).start()
+
+    def result_far(k):
+        res_near_far(k).wait_recv()
+        summed = y_all[target_of(k), quarter_of(far), :].astype(F32) + near_recv[k, 1].astype(F32)
+        y_all[target_of(k), quarter_of(far), :] = summed.astype(BF16)
+        res_far(k).start()
+
+    def result_sum(k):
+        res_near(k).wait_recv()
+        res_far(k).wait_recv()
+        return (
+            y_all[target_of(k), mine, :].astype(F32)
+            + near_recv[k, 0].astype(F32)
+            + far_recv[k].astype(F32)
+        )
+
+    def result_out(k):
+        y_all[target_of(k), mine, :] = result_sum(k).astype(BF16)
+        res_copy(k).start()
+
+    staged((result_step, result_far, result_out), 1)
+
+    result_step(0)
+    in_dd.wait()
+    peers(lambda k: unit_copy(k).wait_recv())
+
+    def down_rows(c):
+        hidden_units = unit_all[pl.ds(c * per_chunk, per_chunk)].reshape(chunk, units)
+        fin_send[row_slice(c), :] = dot(hidden_units, wdd[...]).astype(BF16)
+
+    each(chunks, down_rows)
+
+    def fin_copy(k):
+        return tp_copy(
+            2, k, fin_send.at[quarter_of(lax.rem(mt + k, tn)), :], fin_recv.at[k - 1]
+        )
+
+    tp_peers(lambda k: fin_copy(k).start())
+    result_far(0)
+    dense = fin_send[mine, :].astype(F32)
+    for k in range(1, tn):
+        fin_copy(k).wait_recv()
+        dense = dense + fin_recv[k - 1].astype(F32)
+    gates = []
+    for j in range(pieces):
+        columns = jnp.concatenate([stat_total[j], jnp.zeros((120, 128), F32)], axis=0).T
+        scale = lax.rsqrt(pick_lane(columns, 0) / d_model + EPSILON)
+        gates.append(jax.nn.sigmoid(scale * pick_lane(columns, 1))[0:piece])
+    gate = gates[0] if pieces == 1 else jnp.concatenate(gates, axis=0)
+    out_acc[...] = result_sum(0) + gate * dense
+
+    def take_result(k):
+        res_copy(k).wait_recv()
+        out_acc[...] += res_recv[k - 1].astype(F32)
+
+    peers(take_result)
+    fin_all[mine, :] = (hid_own[...] + out_acc[...]).astype(BF16)
+
+    def all_copy(k):
+        return tp_copy(3, k, fin_all.at[mine, :], fin_all.at[mine, :])
+
+    tp_peers(lambda k: all_copy(k).start())
+    tp_peers(lambda k: all_copy(k).wait_recv())
+    layer_copy = pltpu.make_async_copy(fin_all, layer_out, input_sem.at[15])
+    layer_copy.start()
+    max_copy.wait()
+    norm_copy.wait()
+    state_out.wait()
+    for copies in (
+        proj_copy,
+        gate_copy,
+        heads_copy,
+        stat_copy,
+        dense_copy,
+        unit_copy,
+        res_copy,
+    ):
+        peers(lambda k, copies=copies: copies(k).wait_send())
+    for copies in (res_near, res_near_far, res_far):
+        each(n, lambda k, copies=copies: copies(k).wait_send())
+    for copies in (mix_copy, stat_tp, fin_copy, all_copy):
+        tp_peers(lambda k, copies=copies: copies(k).wait_send())
+    layer_copy.wait()
+
+
+def finish_kernel(parts, layer_in, matrix_in, norm_in, max_in, layer_out, matrix_out, norm_out, max_out, layer_v, matrix_v, norm_v, max_v, in_sem, out_sem):
+    seqs = matrix_in.shape[0] // parts
+    pairs = [
+        (matrix_in.at[pl.ds(i * seqs, seqs)], matrix_v.at[pl.ds(i * seqs, seqs)], matrix_out.at[pl.ds(i * seqs, seqs)])
+        for i in range(parts)
+    ] + [(layer_in, layer_v, layer_out), (norm_in, norm_v, norm_out), (max_in, max_v, max_out)]
+    into = [pltpu.make_async_copy(src, held, in_sem.at[i]) for i, (src, held, _) in enumerate(pairs)]
+    out = [pltpu.make_async_copy(held, dst, out_sem.at[i]) for i, (_, held, dst) in enumerate(pairs)]
+    for copy in into:
+        copy.start()
+    for first, second in zip(into, out):
+        first.wait()
+        second.start()
+    for copy in out:
+        copy.wait()
+
+
+def finish(layer_out, new_matrix, new_norm, new_max):
+    parts = 8
+    arrays = (layer_out, new_matrix, new_norm, new_max)
+    hbm = pl.BlockSpec(memory_space=pl.ANY)
+    return pl.pallas_call(
+        functools.partial(finish_kernel, parts),
+        out_shape=tuple(jax.ShapeDtypeStruct(a.shape, a.dtype) for a in arrays),
+        in_specs=[hbm] * 4,
+        out_specs=(hbm,) * 4,
+        scratch_shapes=[pltpu.VMEM(a.shape, a.dtype) for a in arrays]
+        + [pltpu.SemaphoreType.DMA((parts + 3,)), pltpu.SemaphoreType.DMA((parts + 3,))],
+        compiler_params=pltpu.CompilerParams(vmem_limit_bytes=66_900_000),
+    )(*arrays)
+
+def on_device(
+    n,
+    tn,
+    tokens,
+    mix_gain,
+    w_query,
+    w_key,
+    w_value,
+    w_outgate,
+    w_igate,
+    w_fgate,
+    igate_bias,
+    fgate_bias,
+    head_gain,
+    w_mixout,
+    state_matrix,
+    state_norm,
+    state_max,
+    ffn_gain,
+    dense_mix,
+    w_dense_gate,
+    w_dense_up,
+    w_dense_down,
+    routes,
+    route_weights,
+    w_exp_gate,
+    w_exp_up,
+    w_exp_down,
+):
+    rows, feats = tokens.shape
+    seqs, heads, dk, dv = state_matrix.shape
+    hk, hv = heads * dk, heads * dv
+    units = w_dense_gate.shape[1]
+    wide = 2 * hk + 2 * hv
+    quarter = rows // tn
+    pieces = max(1, quarter // 128)
+    hbm = pl.BlockSpec(memory_space=pl.ANY)
+    dma = pltpu.SemaphoreType.DMA
+    scratch = [
+        pltpu.VMEM(tokens.shape, BF16),
+        pltpu.VMEM(mix_gain.shape, BF16),
+        pltpu.VMEM((heads, feats), BF16),
+        pltpu.VMEM((heads, feats), BF16),
+        pltpu.SMEM(igate_bias.shape, F32),
+        pltpu.SMEM(fgate_bias.shape, F32),
+        pltpu.VMEM(head_gain.shape, BF16),
+        pltpu.VMEM(state_norm.shape, F32),
+        pltpu.VMEM((heads, seqs), F32),
+        pltpu.VMEM(ffn_gain.shape, BF16),
+        pltpu.VMEM(dense_mix.shape, BF16),
+        pltpu.VMEM((routes.shape[1], rows), jnp.int32),
+        pltpu.VMEM((routes.shape[1], rows), F32),
+        pltpu.VMEM(state_norm.shape, F32),
+        pltpu.VMEM((heads, seqs), F32),
+        pltpu.VMEM(w_query.shape, BF16),
+        pltpu.VMEM(w_key.shape, BF16),
+        pltpu.VMEM(w_value.shape, BF16),
+        pltpu.VMEM(w_outgate.shape, BF16),
+        pltpu.VMEM(w_mixout.shape, BF16),
+        pltpu.VMEM(state_matrix.shape, F32),
+        pltpu.VMEM(w_dense_gate.shape, BF16),
+        pltpu.VMEM(w_dense_up.shape, BF16),
+        pltpu.VMEM(w_dense_down.shape, BF16),
+        pltpu.VMEM(w_exp_gate.shape[1:], BF16),
+        pltpu.VMEM(w_exp_up.shape[1:], BF16),
+        pltpu.VMEM((n, units, feats), BF16),
+        pltpu.VMEM((n, seqs, wide), BF16),
+        pltpu.VMEM((n - 1, seqs, wide), BF16),
+        pltpu.VMEM((n, seqs, 128), F32),
+        pltpu.VMEM((n - 1, seqs, 128), F32),
+        pltpu.VMEM((seqs, wide), F32),
+        pltpu.VMEM((n, seqs, hv), BF16),
+        pltpu.VMEM((rows, feats), BF16),
+        pltpu.VMEM((tn - 1, quarter, feats), BF16),
+        pltpu.VMEM((quarter, feats), F32),
+        pltpu.VMEM((n, rows, feats), BF16),
+        pltpu.VMEM((pieces, 8, 128), F32),
+        pltpu.VMEM((n - 1, pieces, 8, 128), F32),
+        pltpu.VMEM((tn, pieces, 8, 128), F32),
+        pltpu.VMEM((rows, 128), F32),
+        pltpu.VMEM((n, seqs, 2 * units), BF16),
+        pltpu.VMEM((n - 1, seqs, 2 * units), BF16),
+        pltpu.VMEM((n, seqs, units), BF16),
+        pltpu.VMEM((rows, 2 * units), F32),
+        pltpu.VMEM((n, 2, quarter, feats), BF16),
+        pltpu.VMEM((n, quarter, feats), BF16),
+        pltpu.VMEM((n - 1, quarter, feats), BF16),
+        pltpu.VMEM((quarter, feats), F32),
+        pltpu.VMEM((rows, feats), BF16),
+        pltpu.VMEM((tn - 1, quarter, feats), BF16),
+        pltpu.VMEM((rows, feats), BF16),
+        pltpu.VMEM((seqs, hk), F32),
+        pltpu.VMEM((128, 128), F32),
+        dma((16,)),
+        dma((12,)),
+        dma((n,)),
+        dma((8, n - 1)),
+        dma((8, n - 1)),
+        dma((4, tn - 1)),
+        dma((4, tn - 1)),
+        dma((6, n)),
+        dma((6, n)),
+    ]
+    layer_out, new_matrix, new_norm, new_max = pl.pallas_call(
+        functools.partial(layer_kernel, n, tn, n * feats),
+        out_shape=(
+            jax.ShapeDtypeStruct((rows, feats), BF16),
+            jax.ShapeDtypeStruct(state_matrix.shape, F32),
+            jax.ShapeDtypeStruct(state_norm.shape, F32),
+            jax.ShapeDtypeStruct((heads, seqs), F32),
+        ),
+        in_specs=[hbm] * 25,
+        out_specs=(hbm,) * 4,
+        scratch_shapes=scratch,
+        compiler_params=pltpu.CompilerParams(
+            collective_id=0, has_side_effects=True, vmem_limit_bytes=66_900_000
+        ),
+    )(
+        tokens,
+        mix_gain,
+        w_query,
+        w_key,
+        w_value,
+        w_outgate,
+        w_igate.T,
+        w_fgate.T,
+        igate_bias,
+        fgate_bias,
+        head_gain,
+        w_mixout,
+        state_matrix,
+        state_norm,
+        state_max.T,
+        ffn_gain,
+        dense_mix,
+        w_dense_gate,
+        w_dense_up,
+        w_dense_down,
+        routes.T,
+        route_weights.T,
+        w_exp_gate,
+        w_exp_up,
+        w_exp_down,
+    )
+    layer_out, new_matrix, new_norm, new_max = finish(layer_out, new_matrix, new_norm, new_max)
+    return layer_out, new_matrix, new_norm, new_max.T
+
+
+def wide_kernel(
     n,
     tn,
     d_model,
@@ -619,7 +1465,7 @@
         tp_peers(lambda k, copies=copies: copies(k).wait_send())
 
 
-def on_device(
+def wide_on_device(
     n,
     tn,
     tokens,
@@ -722,7 +1568,7 @@
         dma((6, n)),
     ]
     layer_out, new_matrix, new_norm, new_max = pl.pallas_call(
-        functools.partial(layer_kernel, n, tn, n * feats),
+        functools.partial(wide_kernel, n, tn, n * feats),
         out_shape=(
             jax.ShapeDtypeStruct((rows, feats), BF16),
             jax.ShapeDtypeStruct(state_matrix.shape, F32),
@@ -764,9 +1610,14 @@
     )
 
 
+def either(n, tn, tokens, *rest):
+    part = on_device if tokens.shape[1] % 128 == 0 else wide_on_device
+    return part(n, tn, tokens, *rest)
+
+
 def solution(mesh):
     return jax.shard_map(
-        functools.partial(on_device, mesh.shape["ep"], mesh.shape["tp"]),
+        functools.partial(either, mesh.shape["ep"], mesh.shape["tp"]),
         mesh=mesh,
         in_specs=(
             P(None, "ep"),

time: 87.5 us -> 76.1 us (0.87)
  local copies, waits for them, and re-layouts: 8.04 us -> 0 us
  other arithmetic: 4.79 us -> 0 us
  Pallas kernels: 73.6 us -> 75.3 us
    unnamed x5 -> x0, local copies, waits for them, and re-layouts: 5.31 us -> none
    convert_element_type x4 -> x0, other arithmetic: 2.73 us -> none  [on_device(): wide_row = jnp.pad(row.astype(F32), (0, width - row.shape[0]))]
    pallas_call x0 -> x1, Pallas kernels: none -> 2.49 us  [finish(): pl.pallas_call(functools.partial(finish_kernel, parts), out_shape=tuple((...]
    reshape x1 -> x0, local copies, waits for them, and re-layouts: 1.41 us -> none  [on_device(): return (layer_out, new_matrix, new_norm.reshape(seqs, heads, dk), new_max.T)]
    concatenate x1 -> x0, other arithmetic: 1.37 us -> none  [on_device(): jnp.concatenate([w_igate.T, w_fgate.T], axis=0)]
    pad x2 -> x0, local copies, waits for them, and re-layouts: 1.32 us -> none  [on_device(): wide_row = jnp.pad(row.astype(F32), (0, width - row.shape[0]))]
where the time goes in v1:
time: 76.1 us; the launch traced here: 76 us
  Pallas kernels  75.3 us (99%)
    pallas_call x1, Pallas kernels, on_device(): pl.pallas_call(functools.partial(layer_kernel, n, tn, n * feats), out_sha...  72.8 us
    pallas_call x1, Pallas kernels, finish(): pl.pallas_call(functools.partial(finish_kernel, parts), out_shape=tuple((...  2.49 us

profile of v1, /device:TPU:29, one launch (start us, length us, event | category | flops | bytes accessed | tf_op | source)
XLA Modules:
  0.0 76.0 jit_solution(553580183568834047)
XLA Ops:
  0.6 72.8 %shard_map.264 = (bf16[128,512]{1,0:T(8,128)(2,1)}, f32[16,4,64,128]{3,2,1,0:T(8,128)}, f32[16,4,64]{2,1,0:T(4,128)}, f32[4,16]{1,0:T(4,128)}) custom-call(bf16[128,512]{1,0:T(8,128)(2,1)} %tokens_in.1, bf16[512]{0:T(512)(128)(2,1)} %mix_gain_in.1, bf16[512,256]{1,0:T(8,128)(2,1)} %w_query.1, bf16[512,256]{1,0:T(8,128)(2,1)} %w_key.1, ...), custom_call_target="tpu_custom_call" | custom-call | tf_op jit(solution)/shard_map/pallas_call | solution.py:838
  73.5 2.5 %shard_map.265 = (bf16[128,512]{1,0:T(8,128)(2,1)}, f32[16,4,64,128]{3,2,1,0:T(8,128)}, f32[16,4,64]{2,1,0:T(4,128)}, f32[4,16]{1,0:T(4,128)}) custom-call(bf16[128,512]{1,0:T(8,128)(2,1)} %get-tuple-element.12.layer_in, f32[16,4,64,128]{3,2,1,0:T(8,128)} %get-tuple-element.13.matrix_in, f32[16,4,64]{2,1,0:T(4,128)} %get-tuple-element.14.norm_in, ...), custom_call_target="tpu_custom_call" | custom-call | tf_op jit(solution)/shard_map/pallas_call | solution.py:725

commit v2 on v0

--- a/solution.py
+++ b/solution.py
@@ -34,7 +34,790 @@
     return jnp.sum(jnp.where(lanes == lane, x, 0.0), axis=1, keepdims=True)
 
 
+def flip(index, mask):
+    bit = 1
+    while bit <= mask:
+        if mask & bit:
+            index = index + bit - 2 * bit * (index // bit % 2)
+        bit *= 2
+    return index
+
+
 def layer_kernel(
+    n,
+    tn,
+    d_model,
+    tokens_in,
+    mix_gain_in,
+    w_query,
+    w_key,
+    w_value,
+    w_outgate,
+    w_igate_in,
+    w_fgate_in,
+    igate_bias_in,
+    fgate_bias_in,
+    head_gain_in,
+    w_mixout,
+    state_matrix,
+    state_norm_in,
+    state_max_in,
+    ffn_gain_in,
+    dense_mix_in,
+    w_dense_gate,
+    w_dense_up,
+    w_dense_down,
+    routes_in,
+    route_weights_in,
+    w_exp_gate,
+    w_exp_up,
+    w_exp_down,
+    layer_out,
+    new_matrix,
+    new_norm,
+    new_max,
+    tokens,
+    mix_gain_v,
+    w_igate,
+    w_fgate,
+    igate_bias,
+    fgate_bias,
+    head_gain_v,
+    state_norm,
+    state_max,
+    ffn_gain_v,
+    dense_mix_v,
+    routes,
+    route_weights,
+    norm_out,
+    max_out,
+    wq,
+    wk,
+    wv,
+    wo,
+    wm,
+    sm,
+    wdg,
+    wdu,
+    wdd,
+    weg,
+    weu,
+    wed,
+    proj_send,
+    pair_proj,
+    line_send,
+    line_proj,
+    proj_acc,
+    heads_all,
+    mix_send,
+    mix_recv,
+    hid_own,
+    y_all,
+    stat_send,
+    stat_recv,
+    stat_all,
+    inv_two,
+    dense_send,
+    dense_recv,
+    unit_all,
+    exp_acc,
+    res_all,
+    near_recv,
+    far_first,
+    pair_first,
+    pair_second,
+    far_second,
+    line_res,
+    fin_send,
+    fin_recv,
+    fin_all,
+    norm_wide,
+    square,
+    local_sem,
+    down_sem,
+    send_sem,
+    recv_sem,
+):
+    me = lax.axis_index("ep")
+    mt = lax.axis_index("tp")
+    rows, feats = tokens_in.shape
+    seqs = state_norm_in.shape[0]
+    heads, dk, dv = sm.shape[1], sm.shape[2], sm.shape[3]
+    hk, hv = heads * dk, heads * dv
+    wide = 2 * hk + 2 * hv
+    units = wdg.shape[1]
+    quarter = rows // tn
+    half = quarter // 2
+    lines = n // 2
+    line, side = me // 2, me % 2
+    near, far, both = flip(mt, 1), flip(mt, 2), flip(mt, 3)
+    started = []
+
+
+    def fetch(src, dst):
+        copy = pltpu.make_async_copy(src, dst, local_sem.at[len(started)])
+        copy.start()
+        started.append(copy)
+        return copy
+
+    first_inputs = [
+        fetch(src, dst)
+        for src, dst in (
+            (tokens_in, tokens),
+            (mix_gain_in, mix_gain_v),
+            (w_igate_in, w_igate),
+            (w_fgate_in, w_fgate),
+            (w_query, wq),
+            (w_key, wk),
+            (w_value, wv),
+            (w_outgate, wo),
+        )
+    ]
+
+    barrier = pltpu.get_barrier_semaphore()
+
+    def ep_flip(k):
+        return flip(me, k)
+
+    for k in range(1, n):
+        pl.semaphore_signal(
+            barrier, inc=1, device_id={"ep": ep_flip(k)}, device_id_type=MESH
+        )
+    for k in range(1, tn):
+        pl.semaphore_signal(
+            barrier, inc=1, device_id={"tp": flip(mt, k)}, device_id_type=MESH
+        )
+
+    in_s = fetch(state_matrix, sm)
+    later_inputs = [
+        fetch(src, dst)
+        for src, dst in (
+            (igate_bias_in, igate_bias),
+            (fgate_bias_in, fgate_bias),
+            (head_gain_in, head_gain_v),
+            (state_norm_in, state_norm),
+            (state_max_in, state_max),
+            (ffn_gain_in, ffn_gain_v),
+            (dense_mix_in, dense_mix_v),
+            (routes_in, routes),
+            (route_weights_in, route_weights),
+        )
+    ]
+    in_m = fetch(w_mixout, wm)
+    in_dg = fetch(w_dense_gate, wdg)
+    in_du = fetch(w_dense_up, wdu)
+    in_dd = fetch(w_dense_down, wdd)
+    in_eg = fetch(w_exp_gate.at[0], weg)
+    in_eu = fetch(w_exp_up.at[0], weu)
+
+    def down_copy(t):
+        src = w_exp_down.at[0, :, pl.ds(pl.multiple_of(t * feats, 128), feats)]
+        return pltpu.make_async_copy(src, wed.at[t], down_sem.at[t])
+
+    for t in range(n):
+        down_copy(t).start()
+
+    sent = []
+
+    def remote(device, src, dst):
+        at = len(sent)
+        copy = pltpu.make_async_remote_copy(
+            src_ref=src,
+            dst_ref=dst,
+            send_sem=send_sem.at[at],
+            recv_sem=recv_sem.at[at],
+            device_id=device,
+            device_id_type=MESH,
+        )
+        sent.append(copy)
+        copy.start()
+        return copy
+
+    def to_ep(k):
+        return {"ep": ep_flip(k)}
+
+    def to_tp(k):
+        return {"tp": flip(mt, k)}
+
+    def group(j, other):
+        return flip(line, j) * 2 + (1 - side if other else side)
+
+    def quarter_of(t):
+        return pl.ds(pl.multiple_of(t * quarter, quarter), quarter)
+
+    def half_of(t, second):
+        return pl.ds(pl.multiple_of(t * quarter + second * half, half), half)
+
+    far_lines = list(range(lines - 1, 0, -1))
+
+    for copy in first_inputs:
+        copy.wait()
+    mix_gain = mix_gain_v[...].astype(F32).reshape(1, feats)
+    gate_weights = jnp.concatenate(
+        [w_igate[...].astype(F32), w_fgate[...].astype(F32), jnp.zeros((128 - 2 * heads, feats), F32)],
+        axis=0,
+    ).astype(BF16)
+    tok = tokens[...].astype(F32)
+    scaled = (tok * mix_gain).astype(BF16)
+    squares = jnp.sum(tok * tok, axis=1, keepdims=True)
+
+    def split_gates(total):
+        high = total.astype(BF16).astype(F32)
+        return (high + pltpu.roll((total - high).astype(BF16).astype(F32), 64, 1)).astype(BF16)
+
+    lanes = lax.broadcasted_iota(jnp.int32, (rows, 128), 1)
+    gates = lax.dot_general(
+        scaled, gate_weights, (((1,), (1,)), ((), ())), preferred_element_type=F32
+    ) + jnp.where(lanes == 2 * heads, squares, 0.0)
+    proj_send[:, :, wide : wide + 128] = split_gates(gates).reshape(n, seqs, 128)
+    offset = 0
+    for weight in (wq, wk, wv, wo):
+        width = weight.shape[1]
+        part = dot(scaled, weight[...]).reshape(n, seqs, width)
+        proj_send[:, :, offset : offset + width] = part.astype(BF16)
+        offset += width
+    pl.semaphore_wait(barrier, n + tn - 2)
+    pair_copies = {
+        j: remote(to_ep(1), proj_send.at[group(j, True)], pair_proj.at[j])
+        for j in far_lines + [0]
+    }
+    line_copies = {}
+    for j in far_lines:
+        pair_copies[j].wait_recv()
+        total = proj_send[group(j, False)].astype(F32) + pair_proj[j].astype(F32)
+        line_send[j - 1, :, 0:wide] = total[:, 0:wide].astype(BF16)
+        packed = total[:, wide:]
+        line_send[j - 1, :, wide:] = split_gates(
+            jnp.where(lanes[0:seqs] < 64, packed + pltpu.roll(packed, 64, 1), 0.0)
+        )
+        line_copies[j] = remote(to_ep(2 * j), line_send.at[j - 1], line_proj.at[j - 1])
+    for copy in later_inputs:
+        copy.wait()
+    bias_lane = lax.broadcasted_iota(jnp.int32, (1, 128), 1)
+    in_bias = jnp.zeros((1, 128), F32)
+    forget_bias = jnp.zeros((1, 128), F32)
+    for h in range(heads):
+        in_bias = jnp.where(bias_lane == h, igate_bias[h], in_bias)
+        forget_bias = jnp.where(bias_lane == h, fgate_bias[h], forget_bias)
+    head_gain = head_gain_v[...].astype(F32).reshape(1, hv)
+    ffn_gain = ffn_gain_v[...].astype(F32).reshape(1, feats)
+    dense_mix = dense_mix_v[...].astype(F32).reshape(1, feats)
+    pair_copies[0].wait_recv()
+    proj_acc[...] = proj_send[me].astype(F32) + pair_proj[0].astype(F32)
+    for j in reversed(far_lines):
+        line_copies[j].wait_recv()
+        proj_acc[...] += line_proj[j - 1].astype(F32)
+    packed = proj_acc[:, wide:]
+    gate_total = packed + pltpu.roll(packed, 64, 1)
+    inverse = lax.rsqrt(pick_lane(gate_total, 2 * heads) / d_model + EPSILON)
+    gate_total = gate_total * inverse
+    in_log = SOFT_CAP * jnp.tanh((gate_total + in_bias) / SOFT_CAP)
+    forget_pre = pltpu.roll(gate_total, 128 - heads, 1)
+    capped = SOFT_CAP * jnp.tanh((forget_pre + forget_bias) / SOFT_CAP)
+    forget_log = jnp.minimum(capped, 0.0) - jnp.log1p(jnp.exp(-jnp.abs(capped)))
+    square[...] = jnp.zeros_like(square)
+    square[0:heads, 0:seqs] = state_max[...]
+    moved = forget_log + square[...].T[0:seqs, :]
+    top = jnp.maximum(moved, in_log)
+    carried = jnp.exp(moved - top)
+    fresh = jnp.exp(in_log - top)
+    floor = jnp.exp(-top)
+    top_square = jnp.concatenate([top, jnp.zeros((128 - seqs, 128), F32)], axis=0).T
+    max_out[...] = top_square[0:heads, 0:seqs]
+    max_copy = pltpu.make_async_copy(max_out, new_max, local_sem.at[25])
+    max_copy.start()
+    head_lane = lax.broadcasted_iota(jnp.int32, (seqs, hk), 1) // dk
+    carried_cols = [pick_lane(carried, h) for h in range(heads)]
+    floor_cols = [pick_lane(floor, h) for h in range(heads)]
+    carried_wide = jnp.zeros((seqs, hk), F32)
+    fresh_wide = jnp.zeros((seqs, hk), F32)
+    for h in range(heads):
+        carried_wide = jnp.where(head_lane == h, carried_cols[h], carried_wide)
+        fresh_wide = jnp.where(head_lane == h, pick_lane(fresh, h), fresh_wide)
+
+    def rounded(lo, width):
+        return (proj_acc[:, lo : lo + width] * inverse).astype(BF16).astype(F32)
+
+    query = rounded(0, hk) * dk ** (-0.5)
+    key = rounded(hk, hk) * fresh_wide
+    value = rounded(2 * hk, hv)
+    outgate = rounded(2 * hk + hv, hv)
+    for h in range(heads):
+        norm_wide[:, h * dk : (h + 1) * dk] = state_norm[:, h, :]
+    norm = carried_wide * norm_wide[...] + key
+    for h in range(heads):
+        norm_out[:, h, :] = norm[:, h * dk : (h + 1) * dk]
+    norm_copy = pltpu.make_async_copy(norm_out, new_norm, local_sem.at[26])
+    norm_copy.start()
+    product = norm * query
+    padding = jnp.zeros((128 - seqs, hk), F32)
+    query_t = jnp.concatenate([query, padding], axis=0).T
+    key_t = jnp.concatenate([key, padding], axis=0).T
+    in_s.wait()
+    for h in range(heads):
+        hs = slice(h * dk, (h + 1) * dk)
+        readouts = []
+        for r in range(seqs):
+            state = (
+                carried_cols[h][r : r + 1, :] * sm[r, h]
+                + key_t[hs, r : r + 1] * value[r : r + 1, h * dv : (h + 1) * dv]
+            )
+            sm[r, h] = state
+            readouts.append(jnp.sum(state * query_t[hs, r : r + 1], axis=0, keepdims=True))
+        numerator = jnp.concatenate(readouts, axis=0)
+        denominator = jnp.sum(jnp.where(head_lane == h, product, 0.0), axis=1, keepdims=True)
+        readout = numerator / jnp.maximum(jnp.abs(denominator), floor_cols[h])
+        cols = slice(h * dv, (h + 1) * dv)
+        scale = lax.rsqrt(jnp.mean(readout * readout, axis=1, keepdims=True) + EPSILON)
+        gated = readout * scale * head_gain[:, cols]
+        gated = gated * jax.nn.sigmoid(outgate[:, cols])
+        heads_all[me, :, cols] = gated.astype(BF16)
+
+    heads_copies = [
+        remote(to_ep(k), heads_all.at[me], heads_all.at[me]) for k in range(n - 1, 0, -1)
+    ]
+    state_out = pltpu.make_async_copy(sm, new_matrix, local_sem.at[27])
+    state_out.start()
+    in_m.wait()
+    for copy in heads_copies:
+        copy.wait_recv()
+    mix_send[...] = dot(heads_all[...].reshape(rows, hv), wm[...]).astype(BF16)
+    mix_copies = [
+        remote(to_tp(k), mix_send.at[quarter_of(flip(mt, k)), :], mix_recv.at[k - 1])
+        for k in range(tn - 1, 0, -1)
+    ]
+    mine = quarter_of(mt)
+    mixed = mix_send[mine, :].astype(F32)
+    for k, copy in zip(range(tn - 1, 0, -1), mix_copies):
+        copy.wait_recv()
+        mixed = mixed + mix_recv[k - 1].astype(F32)
+    hidden = (tokens[mine, :].astype(F32) + mixed.astype(BF16).astype(F32)).astype(BF16)
+    held = hidden.astype(F32)
+    gained = held * ffn_gain
+    y_all[me, mine, :] = gained.astype(BF16)
+
+    def same(device, at, part):
+        view = y_all.at[at, part, :]
+        return remote(device, view, view)
+
+    y_line = {j: same(to_ep(2 * j), me, mine) for j in far_lines}
+    y_pair, y_far, y_near = {}, {}, {}
+    y_pair_far, y_far_pair, y_pair_near, y_far_near, y_last_near = {}, {}, {}, {}, {}
+
+    def spread(j):
+        if j:
+            y_line[j].wait_recv()
+        y_pair[j] = same(to_ep(1), group(j, False), mine)
+        y_far[j] = same(to_tp(2), group(j, False), mine)
+        y_near[j] = same(to_tp(1), group(j, False), mine)
+
+    def second(j):
+        y_pair[j].wait_recv()
+        y_pair_far[j] = same(to_tp(2), group(j, True), half_of(mt, 0))
+        y_pair_near[j] = same(to_tp(1), group(j, True), mine)
+        y_far[j].wait_recv()
+        y_far_pair[j] = same(to_ep(1), group(j, False), half_of(far, 1))
+        y_far_near[j] = same(to_tp(1), group(j, False), quarter_of(far))
+
+    def third(j):
+        y_pair_far[j].wait_recv()
+        y_far_pair[j].wait_recv()
+        y_last_near[j] = same(to_tp(1), group(j, True), quarter_of(far))
+
+    spread(0)
+    hid_own[...] = held
+    squares = jnp.sum(held * held, axis=1, keepdims=True)
+    gate_dot = jnp.sum(gained * dense_mix, axis=1, keepdims=True)
+    lanes = lax.broadcasted_iota(jnp.int32, (quarter, 128), 1)
+    stats = jnp.where(lanes == 0, squares, jnp.where(lanes == 1, gate_dot, 0.0))
+    block = jnp.concatenate([stats, jnp.zeros((128 - quarter, 128), F32)], axis=0)
+    stat_send[...] = block.T[0:8, :]
+    stat_copies = [
+        remote(to_ep(k), stat_send, stat_recv.at[k - 1]) for k in range(n - 1, 0, -1)
+    ]
+
+    def expert_block(source, first):
+        feat_rows = pl.ds(pl.multiple_of(source * feats, feats), feats)
+        held = y_all[source]
+        for lo, weight in ((0, weg), (units, weu)):
+            cols = slice(lo, lo + units)
+            part = dot(held, weight[feat_rows, :])
+            if first:
+                exp_acc[:, cols] = part
+            else:
+                exp_acc[:, cols] += part
+
+    def expert_same(j):
+        y_near[j].wait_recv()
+        y_far_near[j].wait_recv()
+        expert_block(group(j, False), j == 0)
+
+    def expert_other(j):
+        y_pair_near[j].wait_recv()
+        y_last_near[j].wait_recv()
+        expert_block(group(j, True), False)
+
+    spread(1)
+    second(0)
+    for j in range(2, lines):
+        spread(j)
+    in_dg.wait()
+    in_du.wait()
+    y_near[0].wait_recv()
+    y_far_near[0].wait_recv()
+    for lo, weight in ((0, wdg), (units, wdu)):
+        part = dot(y_all[me], weight[...]).reshape(n, seqs, units)
+        dense_send[:, :, lo : lo + units] = part.astype(BF16)
+    dense_copies = [
+        remote(to_ep(k), dense_send.at[ep_flip(k)], dense_recv.at[k - 1])
+        for k in range(n - 1, 0, -1)
+    ]
+    in_eg.wait()
+    in_eu.wait()
+    expert_block(me, True)
+    second(1)
+    third(0)
+    stat_total = stat_send[...]
+    for k, copy in zip(range(n - 1, 0, -1), stat_copies):
+        copy.wait_recv()
+        stat_total = stat_total + stat_recv[k - 1]
+    stat_all[mt] = stat_total
+    stat_tp = [remote(to_tp(k), stat_all.at[mt], stat_all.at[mt]) for k in range(tn - 1, 0, -1)]
+    expert_same(1)
+    expert_other(0)
+    for j in range(2, lines):
+        second(j)
+        third(j - 1)
+        expert_same(j)
+        expert_other(j - 1)
+    third(lines - 1)
+    for copy in stat_tp:
+        copy.wait_recv()
+    for q in range(tn):
+        columns = jnp.concatenate([stat_all[q], jnp.zeros((120, 128), F32)], axis=0).T
+        scale = lax.rsqrt(pick_lane(columns, 0) / d_model + EPSILON)
+        inv_two[q * quarter : (q + 1) * quarter, :] = jnp.broadcast_to(scale, (128, 128))[0:quarter]
+    dense_total = dense_send[me].astype(F32)
+    for k, copy in zip(range(n - 1, 0, -1), dense_copies):
+        copy.wait_recv()
+        dense_total = dense_total + dense_recv[k - 1].astype(F32)
+    seq_scale = inv_two[pl.ds(pl.multiple_of(me * seqs, seqs), seqs), 0:1]
+    dense_total = dense_total * seq_scale
+    unit_all[me] = (
+        jax.nn.silu(dense_total[:, 0:units]) * dense_total[:, units : 2 * units]
+    ).astype(BF16)
+    unit_copies = [
+        remote(to_ep(k), unit_all.at[me], unit_all.at[me]) for k in range(n - 1, 0, -1)
+    ]
+    expert_other(lines - 1)
+    picks = routes[...] == me
+    weight = jnp.sum(jnp.where(picks, route_weights[...], 0.0), axis=0, keepdims=True)
+    weight = pick_lane(jnp.broadcast_to(weight, (rows, rows)).T, 0)
+    scale = inv_two[:, 0:1]
+    gate = exp_acc[:, 0:units] * scale
+    up = exp_acc[:, units : 2 * units] * scale
+    expert_units = (jax.nn.silu(gate) * up * weight).astype(BF16)
+
+    near_copies, far_a, pair_b, pair_a, far_b, line_out = {}, {}, {}, {}, {}, {}
+
+    def compute(j):
+        near_copies[j] = []
+        for other in (True, False):
+            t = group(j, other)
+            down_copy(t).wait()
+            res_all[t] = dot(expert_units, wed[t]).astype(BF16)
+            for slot, q in ((1, both), (0, near)):
+                near_copies[j].append(
+                    remote(
+                        to_tp(1),
+                        res_all.at[t, quarter_of(q), :],
+                        near_recv.at[2 * j + other, slot],
+                    )
+                )
+
+    def add(at, part, other):
+        total = res_all[at, part, :].astype(F32) + other.astype(F32)
+        res_all[at, part, :] = total.astype(BF16)
+
+    def first_sums(j):
+        for copy in near_copies[j]:
+            copy.wait_recv()
+        far_a[j], pair_b[j] = [], []
+        for other in (True, False):
+            t = group(j, other)
+            add(t, quarter_of(far), near_recv[2 * j + other, 1])
+            add(t, mine, near_recv[2 * j + other, 0])
+            far_a[j].append(
+                remote(to_tp(2), res_all.at[t, half_of(far, 0), :], far_first.at[2 * j + other])
+            )
+            if other:
+                for slot, q in ((1, far), (0, mt)):
+                    pair_b[j].append(
+                        remote(
+                            to_ep(1), res_all.at[t, half_of(q, 1), :], pair_first.at[j, slot]
+                        )
+                    )
+
+    def second_sums(j):
+        for copy in far_a[j]:
+            copy.wait_recv()
+        add(group(j, True), half_of(mt, 0), far_first[2 * j + 1])
+        pair_a[j] = remote(
+            to_ep(1), res_all.at[group(j, True), half_of(mt, 0), :], pair_second.at[j]
+        )
+        add(group(j, False), half_of(mt, 0), far_first[2 * j])
+        for copy in pair_b[j]:
+            copy.wait_recv()
+        add(group(j, False), half_of(far, 1), pair_first[j, 1])
+        far_b[j] = remote(
+            to_tp(2), res_all.at[group(j, False), half_of(far, 1), :], far_second.at[j]
+        )
+        add(group(j, False), half_of(mt, 1), pair_first[j, 0])
+
+    def third_sums(j):
+        pair_a[j].wait_recv()
+        add(group(j, False), half_of(mt, 0), pair_second[j])
+        far_b[j].wait_recv()
+        add(group(j, False), half_of(mt, 1), far_second[j])
+        if j:
+            line_out[j] = remote(
+                to_ep(2 * j), res_all.at[group(j, False), mine, :], line_res.at[j - 1]
+            )
+
+    order = far_lines + [0]
+    for j in order:
+        compute(j)
+    for j in order:
+        first_sums(j)
+    for j in order[:-1]:
+        second_sums(j)
+    in_dd.wait()
+    for copy in unit_copies:
+        copy.wait_recv()
+    fin_send[...] = dot(unit_all[...].reshape(rows, units), wdd[...]).astype(BF16)
+    fin_copies = [
+        remote(to_tp(k), fin_send.at[quarter_of(flip(mt, k)), :], fin_recv.at[k - 1])
+        for k in range(tn - 1, 0, -1)
+    ]
+    third_sums(order[0])
+    second_sums(0)
+    for j in order[1:]:
+        third_sums(j)
+    dense = fin_send[mine, :].astype(F32)
+    for k, copy in zip(range(tn - 1, 0, -1), fin_copies):
+        copy.wait_recv()
+        dense = dense + fin_recv[k - 1].astype(F32)
+    columns = jnp.concatenate([stat_total, jnp.zeros((120, 128), F32)], axis=0).T
+    scale = lax.rsqrt(pick_lane(columns, 0) / d_model + EPSILON)
+    gate = jax.nn.sigmoid(scale * pick_lane(columns, 1))[0:quarter]
+    total = hid_own[...] + res_all[me, mine, :].astype(F32) + gate * dense
+    for j in far_lines:
+        line_out[j].wait_recv()
+        total = total + line_res[j - 1].astype(F32)
+    fin_all[mine, :] = total.astype(BF16)
+    all_copies = [
+        remote(to_tp(k), fin_all.at[mine, :], fin_all.at[mine, :]) for k in range(tn - 1, 0, -1)
+    ]
+    outs = []
+
+    def write(at, t):
+        copy = pltpu.make_async_copy(
+            fin_all.at[quarter_of(t), :], layer_out.at[quarter_of(t), :], local_sem.at[28 + at]
+        )
+        copy.start()
+        outs.append(copy)
+
+    write(0, mt)
+    for k, copy in zip(range(tn - 1, 0, -1), all_copies):
+        copy.wait_recv()
+        write(k, flip(mt, k))
+    max_copy.wait()
+    norm_copy.wait()
+    state_out.wait()
+    for copy in sent:
+        copy.wait_send()
+    for copy in outs:
+        copy.wait()
+
+
+def finish_kernel(parts, layer_in, matrix_in, norm_in, max_in, layer_out, matrix_out, norm_out, max_out, layer_v, matrix_v, norm_v, max_v, in_sem, out_sem):
+    seqs = matrix_in.shape[0] // parts
+    pairs = [
+        (matrix_in.at[pl.ds(i * seqs, seqs)], matrix_v.at[pl.ds(i * seqs, seqs)], matrix_out.at[pl.ds(i * seqs, seqs)])
+        for i in range(parts)
+    ] + [(layer_in, layer_v, layer_out), (norm_in, norm_v, norm_out), (max_in, max_v, max_out)]
+    into = [pltpu.make_async_copy(src, held, in_sem.at[i]) for i, (src, held, _) in enumerate(pairs)]
+    out = [pltpu.make_async_copy(held, dst, out_sem.at[i]) for i, (_, held, dst) in enumerate(pairs)]
+    for copy in into:
+        copy.start()
+    for first, second in zip(into, out):
+        first.wait()
+        second.start()
+    for copy in out:
+        copy.wait()
+
+
+def finish(layer_out, new_matrix, new_norm, new_max):
+    parts = 8
+    arrays = (layer_out, new_matrix, new_norm, new_max)
+    hbm = pl.BlockSpec(memory_space=pl.ANY)
+    return pl.pallas_call(
+        functools.partial(finish_kernel, parts),
+        out_shape=tuple(jax.ShapeDtypeStruct(a.shape, a.dtype) for a in arrays),
+        in_specs=[hbm] * 4,
+        out_specs=(hbm,) * 4,
+        scratch_shapes=[pltpu.VMEM(a.shape, a.dtype) for a in arrays]
+        + [pltpu.SemaphoreType.DMA((parts + 3,)), pltpu.SemaphoreType.DMA((parts + 3,))],
+        compiler_params=pltpu.CompilerParams(vmem_limit_bytes=66_900_000),
+    )(*arrays)
+
+def on_device(
+    n,
+    tn,
+    tokens,
+    mix_gain,
+    w_query,
+    w_key,
+    w_value,
+    w_outgate,
+    w_igate,
+    w_fgate,
+    igate_bias,
+    fgate_bias,
+    head_gain,
+    w_mixout,
+    state_matrix,
+    state_norm,
+    state_max,
+    ffn_gain,
+    dense_mix,
+    w_dense_gate,
+    w_dense_up,
+    w_dense_down,
+    routes,
+    route_weights,
+    w_exp_gate,
+    w_exp_up,
+    w_exp_down,
+):
+    rows, feats = tokens.shape
+    seqs, heads, dk, dv = state_matrix.shape
+    hk, hv = heads * dk, heads * dv
+    units = w_dense_gate.shape[1]
+    wide = 2 * hk + 2 * hv
+    quarter = rows // tn
+    hbm = pl.BlockSpec(memory_space=pl.ANY)
+    dma = pltpu.SemaphoreType.DMA
+    lines, half = n // 2, quarter // 2
+    scratch = [
+        pltpu.VMEM(tokens.shape, BF16),
+        pltpu.VMEM(mix_gain.shape, BF16),
+        pltpu.VMEM((heads, feats), BF16),
+        pltpu.VMEM((heads, feats), BF16),
+        pltpu.SMEM(igate_bias.shape, F32),
+        pltpu.SMEM(fgate_bias.shape, F32),
+        pltpu.VMEM(head_gain.shape, BF16),
+        pltpu.VMEM(state_norm.shape, F32),
+        pltpu.VMEM((heads, seqs), F32),
+        pltpu.VMEM(ffn_gain.shape, BF16),
+        pltpu.VMEM(dense_mix.shape, BF16),
+        pltpu.VMEM((routes.shape[1], rows), jnp.int32),
+        pltpu.VMEM((routes.shape[1], rows), F32),
+        pltpu.VMEM(state_norm.shape, F32),
+        pltpu.VMEM((heads, seqs), F32),
+        pltpu.VMEM(w_query.shape, BF16),
+        pltpu.VMEM(w_key.shape, BF16),
+        pltpu.VMEM(w_value.shape, BF16),
+        pltpu.VMEM(w_outgate.shape, BF16),
+        pltpu.VMEM(w_mixout.shape, BF16),
+        pltpu.VMEM(state_matrix.shape, F32),
+        pltpu.VMEM(w_dense_gate.shape, BF16),
+        pltpu.VMEM(w_dense_up.shape, BF16),
+        pltpu.VMEM(w_dense_down.shape, BF16),
+        pltpu.VMEM(w_exp_gate.shape[1:], BF16),
+        pltpu.VMEM(w_exp_up.shape[1:], BF16),
+        pltpu.VMEM((n, units, feats), BF16),
+        pltpu.VMEM((n, seqs, wide + 128), BF16),
+        pltpu.VMEM((lines, seqs, wide + 128), BF16),
+        pltpu.VMEM((lines - 1, seqs, wide + 128), BF16),
+        pltpu.VMEM((lines - 1, seqs, wide + 128), BF16),
+        pltpu.VMEM((seqs, wide + 128), F32),
+        pltpu.VMEM((n, seqs, hv), BF16),
+        pltpu.VMEM((rows, feats), BF16),
+        pltpu.VMEM((tn - 1, quarter, feats), BF16),
+        pltpu.VMEM((quarter, feats), F32),
+        pltpu.VMEM((n, rows, feats), BF16),
+        pltpu.VMEM((8, 128), F32),
+        pltpu.VMEM((n - 1, 8, 128), F32),
+        pltpu.VMEM((tn, 8, 128), F32),
+        pltpu.VMEM((rows, 128), F32),
+        pltpu.VMEM((n, seqs, 2 * units), BF16),
+        pltpu.VMEM((n - 1, seqs, 2 * units), BF16),
+        pltpu.VMEM((n, seqs, units), BF16),
+        pltpu.VMEM((rows, 2 * units), F32),
+        pltpu.VMEM((n, rows, feats), BF16),
+        pltpu.VMEM((n, 2, quarter, feats), BF16),
+        pltpu.VMEM((n, half, feats), BF16),
+        pltpu.VMEM((lines, 2, half, feats), BF16),
+        pltpu.VMEM((lines, half, feats), BF16),
+        pltpu.VMEM((lines, half, feats), BF16),
+        pltpu.VMEM((lines - 1, quarter, feats), BF16),
+        pltpu.VMEM((rows, feats), BF16),
+        pltpu.VMEM((tn - 1, quarter, feats), BF16),
+        pltpu.VMEM((rows, feats), BF16),
+        pltpu.VMEM((seqs, hk), F32),
+        pltpu.VMEM((128, 128), F32),
+        dma((32,)),
+        dma((n,)),
+        dma((160,)),
+        dma((160,)),
+    ]
+    layer_out, new_matrix, new_norm, new_max = pl.pallas_call(
+        functools.partial(layer_kernel, n, tn, n * feats),
+        out_shape=(
+            jax.ShapeDtypeStruct((rows, feats), BF16),
+            jax.ShapeDtypeStruct(state_matrix.shape, F32),
+            jax.ShapeDtypeStruct(state_norm.shape, F32),
+            jax.ShapeDtypeStruct((heads, seqs), F32),
+        ),
+        in_specs=[hbm] * 25,
+        out_specs=(hbm,) * 4,
+        scratch_shapes=scratch,
+        compiler_params=pltpu.CompilerParams(
+            collective_id=0, has_side_effects=True, vmem_limit_bytes=66_900_000
+        ),
+    )(
+        tokens,
+        mix_gain,
+        w_query,
+        w_key,
+        w_value,
+        w_outgate,
+        w_igate.T,
+        w_fgate.T,
+        igate_bias,
+        fgate_bias,
+        head_gain,
+        w_mixout,
+        state_matrix,
+        state_norm,
+        state_max.T,
+        ffn_gain,
+        dense_mix,
+        w_dense_gate,
+        w_dense_up,
+        w_dense_down,
+        routes.T,
+        route_weights.T,
+        w_exp_gate,
+        w_exp_up,
+        w_exp_down,
+    )
+    layer_out, new_matrix, new_norm, new_max = finish(layer_out, new_matrix, new_norm, new_max)
+    return layer_out, new_matrix, new_norm, new_max.T
+
+
+def wide_kernel(
     n,
     tn,
     d_model,
@@ -619,7 +1402,7 @@
         tp_peers(lambda k, copies=copies: copies(k).wait_send())
 
 
-def on_device(
+def wide_on_device(
     n,
     tn,
     tokens,
@@ -722,7 +1505,7 @@
         dma((6, n)),
     ]
     layer_out, new_matrix, new_norm, new_max = pl.pallas_call(
-        functools.partial(layer_kernel, n, tn, n * feats),
+        functools.partial(wide_kernel, n, tn, n * feats),
         out_shape=(
             jax.ShapeDtypeStruct((rows, feats), BF16),
             jax.ShapeDtypeStruct(state_matrix.shape, F32),
@@ -764,9 +1547,15 @@
     )
 
 
+def either(n, tn, tokens, *rest):
+    narrow = tokens.shape[1] % 128 == 0 and tokens.shape[0] == 128 and tn == 4 and n == 8
+    part = on_device if narrow else wide_on_device
+    return part(n, tn, tokens, *rest)
+
+
 def solution(mesh):
     return jax.shard_map(
-        functools.partial(on_device, mesh.shape["ep"], mesh.shape["tp"]),
+        functools.partial(either, mesh.shape["ep"], mesh.shape["tp"]),
         mesh=mesh,
         in_specs=(
             P(None, "ep"),

time: 87.5 us -> 61.5 us (0.70)
  the two profiles are of different devices: /device:TPU:29 before, /device:TPU:0 now
where the time goes in v2:
time: 61.5 us; the launch traced here: 61.4 us
  Pallas kernels  60.7 us (99%)
  between operations  0.65 us (1%)
    pallas_call x1, Pallas kernels, on_device(): pl.pallas_call(functools.partial(layer_kernel, n, tn, n * feats), out_sha...  58.2 us
    pallas_call x1, Pallas kernels, finish(): pl.pallas_call(functools.partial(finish_kernel, parts), out_shape=tuple((...  2.49 us

profile of v2, /device:TPU:0, one launch (start us, length us, event | category | flops | bytes accessed | tf_op | source)
XLA Modules:
  0.0 61.4 jit_solution(2953854308212878488)
XLA Ops:
  0.6 58.2 %shard_map.264 = (bf16[128,512]{1,0:T(8,128)(2,1)}, f32[16,4,64,128]{3,2,1,0:T(8,128)}, f32[16,4,64]{2,1,0:T(4,128)}, f32[4,16]{1,0:T(4,128)}) custom-call(bf16[128,512]{1,0:T(8,128)(2,1)} %tokens_in.1, bf16[512]{0:T(512)(128)(2,1)} %mix_gain_in.1, bf16[512,256]{1,0:T(8,128)(2,1)} %w_query.1, bf16[512,256]{1,0:T(8,128)(2,1)} %w_key.1, ...), custom_call_target="tpu_custom_call" | custom-call | tf_op jit(solution)/shard_map/pallas_call | solution.py:775
  58.9 2.5 %shard_map.265 = (bf16[128,512]{1,0:T(8,128)(2,1)}, f32[16,4,64,128]{3,2,1,0:T(8,128)}, f32[16,4,64]{2,1,0:T(4,128)}, f32[4,16]{1,0:T(4,128)}) custom-call(bf16[128,512]{1,0:T(8,128)(2,1)} %get-tuple-element.12.layer_in, f32[16,4,64,128]{3,2,1,0:T(8,128)} %get-tuple-element.13.matrix_in, f32[16,4,64]{2,1,0:T(4,128)} %get-tuple-element.14.norm_in, ...), custom_call_target="tpu_custom_call" | custom-call | tf_op jit(solution)/shard_map/pallas_call | solution.py:664
